TPU v7x, 256 devices: a whole 4x4x8 slice. The times are simulated.
256 devices in a mesh: dp: 4 (over x), kv: 32 (over z, y), tp: 2 (over core).
Axes of the slice: x: 4, y: 4, z: 8, core: 2. Of those that a mesh axis runs over, the one named last changes fastest.
Arguments:
- tokens: bfloat16 [4, 8192, 1024], P('dp', 'kv', 'tp'), may hold values from -6 to 6
- norm_gain: float32 [1024], replicated, may hold values from 0.1 to 1.9
- w_query: bfloat16 [1024, 1024], P(None, 'tp'), may hold values from -0.1875 to 0.1875
- w_key: bfloat16 [1024, 256], P(None, 'tp'), may hold values from -0.1875 to 0.1875
- w_value: bfloat16 [1024, 256], P(None, 'tp'), may hold values from -0.1875 to 0.1875
- q_gain: float32 [64], replicated, may hold values from 0.1 to 1.9
- k_gain: float32 [64], replicated, may hold values from 0.1 to 1.9
- w_out: bfloat16 [1024, 1024], P('tp'), may hold values from -4 to 4
- chosen: int32 [4, 256, 16], P('dp', 'kv'), may hold values from -1 to 255, as said below
Outputs:
- mixed: bfloat16 [4, 8192, 1024], P('dp', 'kv', 'tp')
- log_total: float32 [4, 16, 8192], P('dp', 'tp', 'kv')
Inputs may be any that keep to these rules, and one draw needn't show every extreme that they name: Each row of chosen (one query block b) holds distinct key block numbers, all at most b, and -1 for empty entries; b itself is always present; a row is full (16 blocks) whenever at least 16 blocks may be chosen by it. Over the 8 rows of one index of kv, the chosen blocks that lie on any one other index of kv are at most 4 distinct ones, and exactly 4 of those on the index just before, for every index but the first. Some blocks are chosen far more often than others.
All inputs are finite; a program needn't handle non-finite values.
Results may differ from a plain program's by a relative error of at most 0.015.
Values may be sent and summed in bfloat16 or wider, within the bound.
A program may use at most 64 MiB of HBM per device.

v0:
```python
import functools
import math

import jax
import jax.numpy as jnp
from jax import lax
from jax.experimental import pallas as pl
from jax.experimental.pallas import tpu as pltpu
from jax.sharding import PartitionSpec as P

HD = 64
BLK = 32
MOST = 4
LANES = 128
PIECES = 3
PARTS = 2

epsilon = 1e-06
alibi_reach = 4.0
masked = -1e30
LOG2E = math.log2(math.e)
F32 = jnp.float32
BF16 = jnp.bfloat16
NT = (((1,), (1,)), ((), ()))


def iota(shape, dim):
    return lax.broadcasted_iota(jnp.int32, shape, dim)


def dot(a, b):
    return jnp.dot(a, b, preferred_element_type=F32)


def dot_nt(a, b):
    return lax.dot_general(a, b, NT, preferred_element_type=F32)


def kernel(
    n_kv,
    tok, gain, wq, wk, wv, qg, kg, wo, ch,
    out_ref, lt_ref,
    x_buf, ch_buf, code_send, code_recv, raw_s, w_buf, wo_buf, g_buf, qg_buf, kg_buf,
    q_s, kv_s, send_s, recv_s, acc, part_send, part_recv,
    load_sem, x_sem, ch_sem, kv_sem, part_sem,
):
    me = lax.axis_index("kv")
    tp = lax.axis_index("tp")
    partner = 1 - tp
    rows, half = tok.shape
    q_cols = wq.shape[1]
    k_cols = wk.shape[1]
    heads = q_cols // HD
    kv_heads = k_cols // HD
    group = heads // kv_heads
    n_heads = heads * lax.axis_size("tp")
    nb = ch.shape[0]
    entries = ch.shape[1]
    nbp = -(-n_kv * nb // LANES) * LANES
    picked = MOST * BLK
    width = half * 2
    seq_len = rows * n_kv
    alibi = alibi_reach / seq_len

    def span(start):
        return pl.ds(pl.multiple_of(start * half, LANES), half)

    loads = {}

    def load(name, src, dst):
        copy = pltpu.make_async_copy(src, dst, load_sem.at[len(loads)])
        copy.start()
        loads[name] = copy

    sides = ((0, tp), (1, partner))
    load("ch", ch, ch_buf)
    load("tok", tok, x_buf.at[0])
    load("g0", gain.at[:, span(tp)], g_buf.at[0])
    for side, which in sides:
        load(f"wk{side}", wk.at[span(which), :], w_buf.at[side, :, q_cols:q_cols + k_cols])
        load(f"wv{side}", wv.at[span(which), :], w_buf.at[side, :, q_cols + k_cols:q_cols + 2 * k_cols])
        load(f"wq{side}", wq.at[span(which), :], w_buf.at[side, :, 0:q_cols])
    load("g1", gain.at[:, span(partner)], g_buf.at[1])
    load("qg", qg, qg_buf)
    load("kg", kg, kg_buf)
    for side, which in sides:
        load(f"wo{side}", wo.at[:, span(which)], wo_buf.at[side])

    def peers(step):
        if n_kv <= 8:
            for d in range(1, n_kv):
                step(d)
        else:
            lax.fori_loop(1, n_kv, lambda d, c: (step(d), c)[1], 0)

    def far_first(step):
        peers(lambda d: step(n_kv - d))

    barrier = pltpu.get_barrier_semaphore()
    pl.semaphore_signal(barrier, inc=1, device_id={"tp": partner}, device_id_type=pl.DeviceIdType.MESH)
    peers(lambda d: pl.semaphore_signal(
        barrier, inc=1, device_id={"kv": lax.rem(me + d, n_kv)}, device_id_type=pl.DeviceIdType.MESH))

    loads["ch"].wait()
    lane_block = iota((nb, nbp), 1)
    lists = ch_buf[...]
    hit = lists[:, 0:1] == lane_block
    for e in range(1, entries):
        hit = hit | (lists[:, e:e + 1] == lane_block)
    member = jnp.where(hit, 1.0, 0.0)
    before = jnp.where(
        (iota((nbp, nbp), 0) < iota((nbp, nbp), 1))
        & (iota((nbp, nbp), 0) // nb == iota((nbp, nbp), 1) // nb), 1.0, 0.0).astype(BF16)
    need = jnp.broadcast_to(jnp.max(member, axis=0, keepdims=True), (8, nbp))
    place = jnp.where(need > 0.5, dot(need.astype(BF16), before), -1.0)

    def place_rows(owner):
        spread = jnp.where(
            iota((nbp, rows), 0) == owner * nb + iota((nbp, rows), 1) // BLK, 1.0, 0.0)
        return dot(place.astype(BF16), spread.astype(BF16))

    def prepare_code(d):
        code_send[d] = place_rows(me - d)

    peers(prepare_code)

    def scaled(side):
        x = x_buf[side].astype(F32)
        return (x * g_buf[side]).astype(BF16), jnp.sum(x * x, axis=1, keepdims=True)

    for name in ("tok", "g0", "wk0", "wv0", "wq0"):
        loads[name].wait()
    y0, sq0 = scaled(0)
    raw_s[...] = dot(y0, w_buf[0])
    pl.semaphore_wait(barrier, n_kv)

    def code_copy(owner, target, d):
        return pltpu.make_async_remote_copy(
            code_send.at[d], code_recv.at[owner], ch_sem.at[0, target], ch_sem.at[1, owner],
            device_id={"kv": target}, device_id_type=pl.DeviceIdType.MESH)

    def send_code(d):
        @pl.when(me - d >= 0)
        def _():
            code_copy(me, lax.max(me - d, 0), d).start()

    peers(send_code)

    x_copy = pltpu.make_async_remote_copy(
        x_buf.at[0], x_buf.at[1], x_sem.at[0], x_sem.at[1],
        device_id={"tp": partner}, device_id_type=pl.DeviceIdType.MESH)
    x_copy.start()

    same_head = jnp.where(
        iota((LANES, LANES), 0) // HD == iota((LANES, LANES), 1) // HD, 1.0, 0.0).astype(BF16)

    def head_norm(v, gain_row):
        sq = v * v
        hi = sq.astype(BF16)
        lo = (sq - hi.astype(F32)).astype(BF16)
        total = dot(hi, same_head) + dot(lo, same_head)
        return v * lax.rsqrt(total / HD + epsilon) * gain_row

    for name in ("g1", "qg", "kg", "wk1", "wv1", "wq1"):
        loads[name].wait()
    qg_row = jnp.concatenate([qg_buf[...], qg_buf[...]], axis=1) * (HD ** -0.5 * LOG2E)
    kg_row = jnp.concatenate([kg_buf[...], kg_buf[...]], axis=1)
    x_copy.wait()
    y1, sq1 = scaled(1)
    row_scale = lax.rsqrt((sq0 + sq1) / width + epsilon)
    raw_kv = (raw_s[:, q_cols:] + dot(y1, w_buf[1, :, q_cols:])) * row_scale
    for tile in range(k_cols // LANES):
        at = tile * LANES
        kv_s[:, at:at + LANES] = head_norm(raw_kv[:, at:at + LANES], kg_row).astype(BF16)
    kv_s[:, k_cols:] = raw_kv[:, k_cols:].astype(BF16)

    same_row = iota((picked, rows), 0) % BLK == iota((picked, rows), 1) % BLK
    row_slot = (iota((picked, rows), 0) // BLK).astype(F32)

    def kv_copy(owner, target, d):
        return pltpu.make_async_remote_copy(
            send_s.at[d], recv_s.at[owner], kv_sem.at[0, target], kv_sem.at[1, owner],
            device_id={"kv": target}, device_id_type=pl.DeviceIdType.MESH)

    def send_rows(d):
        @pl.when(me + d < n_kv)
        def _():
            target = lax.min(me + d, n_kv - 1)
            code_copy(target, me, d).wait_recv()
            code = code_recv[target][0:1]
            chosen_rows = jnp.where(same_row & (code == row_slot), 1.0, 0.0).astype(BF16)
            send_s[d] = dot(chosen_rows, kv_s[...]).astype(BF16)
            kv_copy(me, target, d).start()

    far_first(send_rows)
    raw = (raw_s[:, 0:q_cols] + dot(y1, w_buf[1, :, 0:q_cols])) * row_scale

    lane_q = iota((rows, LANES), 1)
    row_q = iota((rows, LANES), 0)
    own_block = jnp.where(lane_q - HD == row_q // BLK, 1.0, 0.0)

    def slope_of(head):
        return jnp.exp2(-8.0 / n_heads * (tp * heads + head + 1).astype(F32))

    def lane_fill(base, first, value):
        return jnp.where(lane_q == first, value, base)

    for tile in range(q_cols // LANES):
        at = tile * LANES
        q = head_norm(raw[:, at:at + LANES], qg_row)
        for odd in range(2):
            head = 2 * tile + odd
            value = slope_of(jnp.full((rows, LANES), head, jnp.int32)) * (alibi * LOG2E)
            extra = own_block
            for piece in range(PIECES):
                part = value.astype(BF16).astype(F32)
                value = value - part
                extra = lane_fill(extra, HD + nb + piece, part * BLK)
                extra = lane_fill(extra, HD + nb + PIECES + piece, part)
            here = q if odd == 0 else pltpu.roll(q, HD, 1)
            q_s[head] = jnp.where(lane_q < HD, here, extra).astype(BF16)

    relative = (lane_block - me * nb).astype(F32)
    pieces_rows = jnp.where(
        iota((8, nbp), 0) < PIECES,
        jnp.broadcast_to(relative[0:1], (8, nbp)), 0.0)
    table = jnp.concatenate(
        [jnp.zeros((HD, nbp), F32), member, pieces_rows,
         jnp.zeros((LANES - HD - nb - 8, nbp), F32)], axis=0).astype(BF16)

    def key_extra(hot):
        count = hot.shape[0]
        lane = iota((count, LANES), 1)
        found = dot_nt(hot, table)
        inside = (iota((count, LANES), 0) % BLK).astype(F32)
        tail = jnp.where(lane < HD + nb + 2 * PIECES, inside, 0.0)
        tail = jnp.where(lane < HD + nb + PIECES, found, tail)
        return jnp.where(lane < HD + nb, (found - 1.0) * -masked, tail)

    def attend(load_tile, extra, causal, first):
        count = extra.shape[0]
        low = iota((count, LANES), 1) < HD
        for g in range(kv_heads):
            at = g * HD // LANES * LANES
            k = load_tile(at).astype(F32)
            v = load_tile(k_cols + at).astype(F32)
            if g % 2:
                k = pltpu.roll(k, HD, 1)
                v = pltpu.roll(v, HD, 1)
            k = jnp.where(low, k, extra).astype(BF16)
            v = jnp.where(low, v, 1.0).astype(BF16)
            for h in range(g * group, (g + 1) * group):
                weights = jnp.exp2(dot_nt(q_s[h], k))
                if causal is not None:
                    weights = jnp.where(causal, weights, 0.0)
                add = dot(weights.astype(BF16), v)
                if first:
                    acc[h] = add
                else:
                    acc[h] += add

    hot_own = jnp.where(
        iota((rows, nbp), 1) == me * nb + iota((rows, nbp), 0) // BLK, 1.0, 0.0).astype(BF16)
    causal = iota((rows, rows), 1) <= iota((rows, rows), 0)
    attend(lambda at: kv_s[:, at:at + LANES], key_extra(hot_own), causal, True)

    slot = (iota((picked, nbp), 0) // BLK).astype(F32)
    lane_owner = iota((picked, nbp), 1) // nb

    def absorb(d):
        @pl.when(me - d >= 0)
        def _():
            owner = lax.max(me - d, 0)
            hot = jnp.where((place[0:1] == slot) & (lane_owner == owner), 1.0, 0.0)
            extra = key_extra(hot.astype(BF16))
            kv_copy(owner, me, d).wait_recv()
            attend(lambda at: recv_s[owner, :, at:at + LANES], extra, None, False)

    far_first(absorb)

    loads["wo0"].wait()
    loads["wo1"].wait()
    part_rows = rows // PARTS
    low = iota((part_rows, LANES), 1) < HD
    lane = iota((part_rows, LANES), 1)

    def part_copy(part):
        at = pl.ds(part * part_rows, part_rows)
        return pltpu.make_async_remote_copy(
            part_send.at[at], part_recv.at[at], part_sem.at[0, part], part_sem.at[1, part],
            device_id={"tp": partner}, device_id_type=pl.DeviceIdType.MESH)

    attended, all_sums = [], []
    for part in range(PARTS):
        at = slice(part * part_rows, (part + 1) * part_rows)
        sums = jnp.ones((part_rows, LANES), F32)
        tiles = []
        for tile in range(q_cols // LANES):
            pair = []
            for odd in range(2):
                pair.append(acc[2 * tile + odd, at])
            turned = [pltpu.roll(o, HD, 1) for o in pair]
            total = jnp.where(low, turned[0], pair[1])
            tiles.append(jnp.where(low, pair[0], turned[1]) / total)
            for odd in range(2):
                sums = jnp.where(lane == 2 * tile + odd, turned[odd], sums)
        attended.append(jnp.concatenate(tiles, axis=1).astype(BF16))
        all_sums.append(sums)
        part_send[at] = dot(attended[part], wo_buf[1]).astype(BF16)
        part_copy(part).start()

    own = [dot(a, wo_buf[0]) for a in attended]
    logs = jnp.log(jnp.concatenate(all_sums, axis=0))
    logs = logs - slope_of(lane_q) * alibi * row_q.astype(F32)
    lt_ref[...] = logs.T[0:heads]

    def finish(d):
        @pl.when(me + d < n_kv)
        def _():
            kv_copy(me, lax.min(me + d, n_kv - 1), d).wait_send()

        @pl.when(me - d >= 0)
        def _():
            code_copy(me, lax.max(me - d, 0), d).wait_send()

    peers(finish)
    for part in range(PARTS):
        at = slice(part * part_rows, (part + 1) * part_rows)
        part_copy(part).wait()
        out_ref[at] = (own[part] + part_recv[at].astype(F32)).astype(BF16)


def write_out(mixed, log_total, mixed_out, log_out, sems):
    copies = [
        pltpu.make_async_copy(mixed, mixed_out, sems.at[0]),
        pltpu.make_async_copy(log_total, log_out, sems.at[1]),
    ]
    for copy in copies:
        copy.start()
    for copy in copies:
        copy.wait()


def shards(n_kv, tokens, norm_gain, w_query, w_key, w_value, q_gain, k_gain, w_out, chosen):
    seqs, rows, half = tokens.shape
    nb, entries = chosen.shape[1:]
    q_cols, k_cols = w_query.shape[1], w_key.shape[1]
    heads = q_cols // HD
    vmem = pltpu.VMEM
    dma = pltpu.SemaphoreType.DMA
    mixed, log_total = pl.pallas_call(
        functools.partial(kernel, n_kv),
        out_shape=(vmem((rows, half), BF16), vmem((heads, rows), F32)),
        in_specs=[pl.BlockSpec(memory_space=pltpu.HBM)] * 9,
        out_specs=(pl.BlockSpec(memory_space=vmem), pl.BlockSpec(memory_space=vmem)),
        scratch_shapes=[
            vmem((2, rows, half), BF16),
            vmem((nb, entries), jnp.int32),
            vmem((n_kv, 8, rows), F32),
            vmem((n_kv, 8, rows), F32),
            vmem((rows, q_cols + 2 * k_cols), F32),
            vmem((2, half, q_cols + 2 * k_cols), BF16),
            vmem((2, q_cols, half), BF16),
            vmem((2, 1, half), F32),
            vmem((1, HD), F32),
            vmem((1, HD), F32),
            vmem((heads, rows, LANES), BF16),
            vmem((rows, 2 * k_cols), BF16),
            vmem((n_kv, MOST * BLK, 2 * k_cols), BF16),
            vmem((n_kv, MOST * BLK, 2 * k_cols), BF16),
            vmem((heads, rows, LANES), F32),
            vmem((rows, half), BF16),
            vmem((rows, half), BF16),
            dma((14,)),
            dma((2,)),
            dma((2, n_kv)),
            dma((2, n_kv)),
            dma((2, PARTS)),
        ],
        compiler_params=pltpu.CompilerParams(
            collective_id=0, has_side_effects=True, vmem_limit_bytes=66_700_000
        ),
    )(
        tokens.reshape(rows, half), norm_gain.reshape(1, -1), w_query, w_key, w_value,
        q_gain.reshape(1, -1), k_gain.reshape(1, -1), w_out, chosen.reshape(nb, entries),
    )
    mixed, log_total = pl.pallas_call(
        write_out,
        out_shape=(
            jax.ShapeDtypeStruct((rows, half), BF16),
            jax.ShapeDtypeStruct((heads, rows), F32),
        ),
        in_specs=[pl.BlockSpec(memory_space=pl.ANY)] * 2,
        out_specs=(pl.BlockSpec(memory_space=pltpu.HBM),) * 2,
        scratch_shapes=[dma((2,))],
        compiler_params=pltpu.CompilerParams(vmem_limit_bytes=1_000_000),
    )(mixed, log_total)
    return mixed.reshape(seqs, rows, half), log_total.reshape(seqs, heads, rows)


def solution(mesh):
    in_specs = (
        P("dp", "kv", "tp"),
        P(),
        P(None, "tp"),
        P(None, "tp"),
        P(None, "tp"),
        P(),
        P(),
        P("tp", None),
        P("dp", "kv", None),
    )
    out_specs = (P("dp", "kv", "tp"), P("dp", "tp", "kv"))
    return jax.shard_map(
        functools.partial(shards, mesh.shape["kv"]),
        mesh=mesh, in_specs=in_specs, out_specs=out_specs, check_vma=False)
```

profile of v0, /device:TPU:165, one launch (start us, length us, event | category | flops | bytes accessed | tf_op | source)
XLA Modules:
  0.0 85.8 jit_solution(13690548584957422250)
XLA Ops:
  0.6 84.4 %shard_map.104 = (bf16[256,512]{1,0:T(8,128)(2,1)S(1)}, f32[8,256]{1,0:T(8,128)S(1)}) custom-call(bf16[256,512]{1,0:T(8,128)(2,1)} %bitcast.7, f32[1,1024]{1,0:T(1,128)} %bitcast.8, bf16[1024,512]{1,0:T(8,128)(2,1)} %wq.1, bf16[1024,128]{1,0:T(8,128)(2,1)} %wk.1, bf16[1024,128]{1,0:T(8,128)(2,1)} %wv.1, f32[1,64]{1,0:T(1,128)} %bitcast.10, ...), custom_call_target="tpu_custom_call" | custom-call | tf_op jit(solution)/shard_map/pallas_call | solution.py:351
  85.1 0.7 shard_map.105
where the time goes:
time: 85.9 us; the launch traced here: 85.8 us
  Pallas kernels  85.1 us (99%)
    pallas_call x1, Pallas kernels, shards(): pl.pallas_call(functools.partial(kernel, n_kv), out_shape=(vmem((rows, ha...  84.4 us

commit v1 on v0

v1 whole, which is shorter than its diff:
```python
import functools
import math

import jax
import jax.numpy as jnp
from jax import lax
from jax.experimental import pallas as pl
from jax.experimental.pallas import tpu as pltpu
from jax.sharding import PartitionSpec as P

HD = 64
BLK = 32
LANES = 128
PARTS = 2
N_Y = 4
CHUNKS = 2
UP, DOWN, LEFT, RIGHT = range(4)

epsilon = 1e-06
alibi_reach = 4.0
LOG2E = math.log2(math.e)
F32 = jnp.float32
BF16 = jnp.bfloat16
NT = (((1,), (1,)), ((), ()))
MESH = pl.DeviceIdType.MESH


def iota(shape, dim):
    return lax.broadcasted_iota(jnp.int32, shape, dim)


def dot(a, b):
    return jnp.dot(a, b, preferred_element_type=F32)


def dot_nt(a, b):
    return lax.dot_general(a, b, NT, preferred_element_type=F32)


def kernel(
    n_kv,
    tok, gain, wq, wk, wv, qg, kg, wo, ch,
    out_ref, lt_ref,
    x_buf, ch_s, ch_buf, raw_s, w_buf, wo_buf, g_buf, qg_buf, kg_buf,
    q_s, kv_all, kp_s, att_s, sum_s, part_send, part_recv,
    load_sem, x_sem, send_sem, recv_sem, part_sem,
):
    me = lax.axis_index("kv")
    tp = lax.axis_index("tp")
    partner = 1 - tp
    n_z = n_kv // N_Y
    z = me // N_Y
    y = me % N_Y
    rows, half = tok.shape
    q_cols = wq.shape[1]
    k_cols = wk.shape[1]
    heads = q_cols // HD
    kv_heads = k_cols // HD
    group = heads // kv_heads
    n_heads = heads * lax.axis_size("tp")
    nb, entries = ch.shape
    width = half * 2
    seq_len = rows * n_kv
    alibi = alibi_reach / seq_len
    keys = entries * BLK

    def span(start):
        return pl.ds(pl.multiple_of(start * half, LANES), half)

    loads = {}

    def load(name, src, dst):
        copy = pltpu.make_async_copy(src, dst, load_sem.at[len(loads)])
        copy.start()
        loads[name] = copy

    sides = ((0, tp), (1, partner))
    load("tok", tok, x_buf.at[0])
    load("g0", gain.at[:, span(tp)], g_buf.at[0])
    for side, which in sides:
        load(f"wk{side}", wk.at[span(which), :], w_buf.at[side, :, q_cols:q_cols + k_cols])
        load(f"wv{side}", wv.at[span(which), :], w_buf.at[side, :, q_cols + k_cols:q_cols + 2 * k_cols])
        load(f"wq{side}", wq.at[span(which), :], w_buf.at[side, :, 0:q_cols])
    load("g1", gain.at[:, span(partner)], g_buf.at[1])
    load("qg", qg, qg_buf)
    load("kg", kg, kg_buf)
    load("chs", ch, ch_s)
    load("ch", ch, ch_buf)
    for side, which in sides:
        for head in range(heads):
            to = head % group * LANES + head // group * HD
            load(f"wo{side}{head}", wo.at[head * HD:(head + 1) * HD, span(which)],
                 wo_buf.at[side, to:to + HD])

    def device(row, col):
        return lax.rem(row + n_z, n_z) * N_Y + lax.rem(col + N_Y, N_Y)

    neighbour = {
        UP: device(z + 1, y), DOWN: device(z - 1, y),
        LEFT: device(z, y - 1), RIGHT: device(z, y + 1),
    }
    barrier = pltpu.get_barrier_semaphore()
    pl.semaphore_signal(barrier, inc=1, device_id={"tp": partner}, device_id_type=MESH)
    for target in neighbour.values():
        pl.semaphore_signal(barrier, inc=1, device_id={"kv": target}, device_id_type=MESH)

    def scaled(side):
        x = x_buf[side].astype(F32)
        return (x * g_buf[side]).astype(BF16), jnp.sum(x * x, axis=1, keepdims=True)

    loads["tok"].wait()
    pl.semaphore_wait(barrier, 5)
    x_copy = pltpu.make_async_remote_copy(
        x_buf.at[0], x_buf.at[1], x_sem.at[0], x_sem.at[1],
        device_id={"tp": partner}, device_id_type=MESH)
    x_copy.start()

    for name in ("g0", "wk0", "wv0", "wq0"):
        loads[name].wait()
    y0, sq0 = scaled(0)
    raw_s[...] = dot(y0, w_buf[0])

    same_head = jnp.where(
        iota((LANES, LANES), 0) // HD == iota((LANES, LANES), 1) // HD, 1.0, 0.0).astype(BF16)

    def head_norm(v, gain_row):
        sq = v * v
        hi = sq.astype(BF16)
        lo = (sq - hi.astype(F32)).astype(BF16)
        total = dot(hi, same_head) + dot(lo, same_head)
        return v * lax.rsqrt(total / HD + epsilon) * gain_row

    for name in ("g1", "qg", "kg", "wk1", "wv1", "wq1"):
        loads[name].wait()
    qg_row = jnp.concatenate([qg_buf[...], qg_buf[...]], axis=1) * (HD ** -0.5 * LOG2E)
    kg_row = jnp.concatenate([kg_buf[...], kg_buf[...]], axis=1)
    x_copy.wait()
    y1, sq1 = scaled(1)
    row_scale = lax.rsqrt((sq0 + sq1) / width + epsilon)
    raw_kv = (raw_s[:, q_cols:] + dot(y1, w_buf[1, :, q_cols:])) * row_scale
    mine = pl.ds(1 + me * nb, nb)
    kv_all[0] = jnp.zeros((BLK, 2 * k_cols), BF16)
    key_part = head_norm(raw_kv[:, 0:k_cols], kg_row).astype(BF16)
    value_part = raw_kv[:, k_cols:].astype(BF16)
    kv_all[mine] = jnp.concatenate([key_part, value_part], axis=1).reshape(nb, BLK, 2 * k_cols)

    chunk_blocks = nb // CHUNKS
    sent = []

    def kv_copy(direction, owner, chunk):
        at = pl.ds(1 + owner * nb + chunk * chunk_blocks, chunk_blocks)
        return pltpu.make_async_remote_copy(
            kv_all.at[at], kv_all.at[at],
            send_sem.at[direction, chunk, owner], recv_sem.at[chunk, owner],
            device_id={"kv": neighbour[direction]}, device_id_type=MESH)

    def send(direction, owner, chunk, when):
        sent.append((direction, owner, chunk, when))

        @pl.when(when)
        def _():
            kv_copy(direction, owner, chunk).start()

    def arrive(owner, chunk, when):
        @pl.when(when)
        def _():
            kv_copy(UP, owner, chunk).wait_recv()

    last = n_z - 1
    reach_a, reach_b = n_z // 2, n_z // 2 - 1
    back_a, back_b = last - reach_a, last - reach_b
    for chunk in range(CHUNKS):
        send(RIGHT, me, chunk, (z < last) | (y < N_Y - 1))
        send(UP, me, chunk, z < last)
        send(DOWN, me, chunk, z < back_a)
        send(LEFT, me, chunk, y == 0)

    raw = (raw_s[:, 0:q_cols] + dot(y1, w_buf[1, :, 0:q_cols])) * row_scale
    low = iota((rows, LANES), 1) < HD
    for tile in range(q_cols // LANES):
        q = head_norm(raw[:, tile * LANES:(tile + 1) * LANES], qg_row)
        turned = pltpu.roll(q, HD, 1)
        for odd in range(2):
            head = 2 * tile + odd
            side = head // group
            here = q if odd == side else turned
            here = jnp.where(low if side == 0 else ~low, here, 0.0).astype(BF16)
            for r in range(nb):
                q_s[r, head * BLK:(head + 1) * BLK] = here[r * BLK:(r + 1) * BLK]

    loads["ch"].wait()
    loads["chs"].wait()
    lists = ch_buf[...]
    lane = iota((nb, keys), 1)
    block = jnp.full((nb, keys), -1, jnp.int32)
    for e in range(entries):
        block = jnp.where(lane // BLK == e, lists[:, e:e + 1], block)
    away = (block - (me * nb + iota((nb, keys), 0))) * BLK + lane % BLK
    kp_s[...] = jnp.where(block < 0, 1 << 24, away).astype(F32)

    left_col = lax.rem(y + N_Y - 1, N_Y)
    left_me = z * N_Y + left_col
    for chunk in range(CHUNKS):
        arrive(left_me, chunk, (z < last) | (y > 0))
        send(UP, left_me, chunk, z < last)
        send(DOWN, left_me, chunk, z < back_b)
        send(RIGHT, left_me, chunk, (y == 1) | (y == 2))

    for hop in range(1, n_z // 2 + 1):
        above = z - hop
        below = lax.rem(z + hop, n_z)
        for col, reach, back, side in ((y, reach_a, back_a, LEFT), (left_col, reach_b, back_b, RIGHT)):
            for chunk in range(CHUNKS):
                if hop <= reach:
                    owner = lax.max(above, 0) * N_Y + col
                    arrive(owner, chunk, above >= 0)
                    if hop < reach:
                        send(UP, owner, chunk, (above >= 0) & (z < last))
                    send(side, owner, chunk, above >= 0)
                if hop <= back:
                    owner = below * N_Y + col
                    valid = below < back
                    arrive(owner, chunk, valid)
                    if hop < back:
                        send(DOWN, owner, chunk, valid)
                    send(side, owner, chunk, valid & (below < z))

    right_col = lax.rem(y + 1, N_Y)
    far_col = lax.rem(y + 2, N_Y)
    for row in range(n_z):
        for chunk in range(CHUNKS):
            arrive(row * N_Y + right_col, chunk, (row < z) | ((row == z) & (y == N_Y - 1)))
            arrive(row * N_Y + far_col, chunk, (row < z) | ((row == z) & (y >= 2)))

    query_row = iota((BLK, keys), 0).astype(F32)
    ones = jnp.ones((keys, LANES), BF16)
    tile_low = iota((BLK, LANES), 1) < HD
    tile_lane = iota((BLK, LANES), 1)
    core_slope = jnp.where(tp == 0, 1.0, 2.0 ** (-8.0 * heads / n_heads)).astype(F32)

    def slope_of(head):
        return core_slope * (2.0 ** (-8.0 * (head + 1) / n_heads))

    def attend(r):
        key_rows, value_rows = [], []
        for e in range(entries):
            tile = kv_all[ch_s[r, e] + 1]
            key_rows.append(tile[:, 0:k_cols])
            value_rows.append(tile[:, k_cols:])
        key_rows = jnp.concatenate(key_rows, axis=0)
        value_rows = jnp.concatenate([jnp.concatenate(value_rows, axis=0), ones], axis=1)
        scores = dot_nt(q_s[r], key_rows)
        key_pos = kp_s[r:r + 1, :]
        allowed = key_pos <= query_row
        weights = []
        for head in range(heads):
            bias = key_pos * (slope_of(head) * (alibi * LOG2E))
            part = jnp.exp2(scores[head * BLK:(head + 1) * BLK] + bias)
            weights.append(jnp.where(allowed, part, 0.0).astype(BF16))
        found = dot(jnp.concatenate(weights, axis=0), value_rows)

        def of(head):
            return found[head * BLK:(head + 1) * BLK]

        sums = jnp.ones((BLK, LANES), F32)
        at = slice(r * BLK, (r + 1) * BLK)
        for t in range(group):
            first, second = of(t), of(t + group)
            top = jnp.where(tile_low, first[:, 0:LANES], second[:, 0:LANES])
            total = jnp.where(tile_low, first[:, LANES:], second[:, LANES:])
            att_s[at, t * LANES:(t + 1) * LANES] = (top / total).astype(BF16)
            sums = jnp.where(tile_lane == t, first[:, LANES:], sums)
            sums = jnp.where(tile_lane == t + group, second[:, LANES:], sums)
        sum_s[at] = sums

    for side in range(2):
        for head in range(heads):
            loads[f"wo{side}{head}"].wait()
    part_rows = rows // PARTS

    def part_copy(part):
        at = pl.ds(part * part_rows, part_rows)
        return pltpu.make_async_remote_copy(
            part_send.at[at], part_recv.at[at], part_sem.at[0, part], part_sem.at[1, part],
            device_id={"tp": partner}, device_id_type=MESH)

    for part in range(PARTS):
        at = slice(part * part_rows, (part + 1) * part_rows)
        for r in range(part * nb // PARTS, (part + 1) * nb // PARTS):
            attend(r)
        part_send[at] = dot(att_s[at], wo_buf[1]).astype(BF16)
        part_copy(part).start()

    own = dot(att_s[...], wo_buf[0])
    row_in = (iota((rows, LANES), 0) % BLK).astype(F32)
    slopes = jnp.exp2(-8.0 / n_heads * (tp * heads + iota((rows, LANES), 1) + 1).astype(F32))
    logs = jnp.log(sum_s[...]) - slopes * alibi * row_in
    lt_ref[...] = logs.T[0:heads]

    for direction, owner, chunk, when in sent:
        @pl.when(when)
        def _():
            kv_copy(direction, owner, chunk).wait_send()

    for part in range(PARTS):
        at = slice(part * part_rows, (part + 1) * part_rows)
        part_copy(part).wait()
        out_ref[at] = (own[at] + part_recv[at].astype(F32)).astype(BF16)


def write_out(mixed, log_total, mixed_out, log_out, sems):
    copies = [
        pltpu.make_async_copy(mixed, mixed_out, sems.at[0]),
        pltpu.make_async_copy(log_total, log_out, sems.at[1]),
    ]
    for copy in copies:
        copy.start()
    for copy in copies:
        copy.wait()


def shards(n_kv, tokens, norm_gain, w_query, w_key, w_value, q_gain, k_gain, w_out, chosen):
    seqs, rows, half = tokens.shape
    nb, entries = chosen.shape[1:]
    q_cols, k_cols = w_query.shape[1], w_key.shape[1]
    heads = q_cols // HD
    vmem = pltpu.VMEM
    dma = pltpu.SemaphoreType.DMA
    mixed, log_total = pl.pallas_call(
        functools.partial(kernel, n_kv),
        out_shape=(vmem((rows, half), BF16), vmem((heads, rows), F32)),
        in_specs=[pl.BlockSpec(memory_space=pltpu.HBM)] * 9,
        out_specs=(pl.BlockSpec(memory_space=vmem), pl.BlockSpec(memory_space=vmem)),
        scratch_shapes=[
            vmem((2, rows, half), BF16),
            pltpu.SMEM((nb, entries), jnp.int32),
            vmem((nb, entries), jnp.int32),
            vmem((rows, q_cols + 2 * k_cols), F32),
            vmem((2, half, q_cols + 2 * k_cols), BF16),
            vmem((2, q_cols, half), BF16),
            vmem((2, 1, half), F32),
            vmem((1, HD), F32),
            vmem((1, HD), F32),
            vmem((nb, heads * BLK, LANES), BF16),
            vmem((1 + n_kv * nb, BLK, 2 * k_cols), BF16),
            vmem((nb, entries * BLK), F32),
            vmem((rows, q_cols), BF16),
            vmem((rows, LANES), F32),
            vmem((rows, half), BF16),
            vmem((rows, half), BF16),
            dma((13 + 2 * heads,)),
            dma((2,)),
            dma((4, CHUNKS, n_kv)),
            dma((CHUNKS, n_kv)),
            dma((2, PARTS)),
        ],
        compiler_params=pltpu.CompilerParams(
            collective_id=0, has_side_effects=True, vmem_limit_bytes=66_700_000
        ),
    )(
        tokens.reshape(rows, half), norm_gain.reshape(1, -1), w_query, w_key, w_value,
        q_gain.reshape(1, -1), k_gain.reshape(1, -1), w_out, chosen.reshape(nb, entries),
    )
    mixed, log_total = pl.pallas_call(
        write_out,
        out_shape=(
            jax.ShapeDtypeStruct((rows, half), BF16),
            jax.ShapeDtypeStruct((heads, rows), F32),
        ),
        in_specs=[pl.BlockSpec(memory_space=pl.ANY)] * 2,
        out_specs=(pl.BlockSpec(memory_space=pltpu.HBM),) * 2,
        scratch_shapes=[dma((2,))],
        compiler_params=pltpu.CompilerParams(vmem_limit_bytes=1_000_000),
    )(mixed, log_total)
    return mixed.reshape(seqs, rows, half), log_total.reshape(seqs, heads, rows)


def solution(mesh):
    in_specs = (
        P("dp", "kv", "tp"),
        P(),
        P(None, "tp"),
        P(None, "tp"),
        P(None, "tp"),
        P(),
        P(),
        P("tp", None),
        P("dp", "kv", None),
    )
    out_specs = (P("dp", "kv", "tp"), P("dp", "tp", "kv"))
    return jax.shard_map(
        functools.partial(shards, mesh.shape["kv"]),
        mesh=mesh, in_specs=in_specs, out_specs=out_specs, check_vma=False)
```

time: 85.9 us -> 41.6 us (0.48)
  the two profiles are of different devices: /device:TPU:165 before, /device:TPU:193 now
where the time goes in v1:
time: 41.6 us; the launch traced here: 41.5 us
  Pallas kernels  40.9 us (98%)
  between operations  0.64 us (2%)
    pallas_call x1, Pallas kernels, shards(): pl.pallas_call(functools.partial(kernel, n_kv), out_shape=(vmem((rows, ha...  40.1 us

profile of v1, /device:TPU:193, one launch (start us, length us, event | category | flops | bytes accessed | tf_op | source)
XLA Modules:
  0.0 41.5 jit_solution(3773290618919414237)
XLA Ops:
  0.6 40.1 %shard_map.104 = (bf16[256,512]{1,0:T(8,128)(2,1)S(1)}, f32[8,256]{1,0:T(8,128)S(1)}) custom-call(bf16[256,512]{1,0:T(8,128)(2,1)} %bitcast.7, f32[1,1024]{1,0:T(1,128)} %bitcast.8, bf16[1024,512]{1,0:T(8,128)(2,1)} %wq.1, bf16[1024,128]{1,0:T(8,128)(2,1)} %wk.1, bf16[1024,128]{1,0:T(8,128)(2,1)} %wv.1, f32[1,64]{1,0:T(1,128)} %bitcast.10, ...), custom_call_target="tpu_custom_call" | custom-call | tf_op jit(solution)/shard_map/pallas_call | solution.py:329
  40.8 0.7 %shard_map.105 = (bf16[256,512]{1,0:T(8,128)(2,1)}, f32[8,256]{1,0:T(8,128)}) custom-call(bf16[256,512]{1,0:T(8,128)(2,1)S(1)} %get-tuple-element.6.mixed, f32[8,256]{1,0:T(8,128)S(1)} %get-tuple-element.7.log_total), custom_call_target="tpu_custom_call" | custom-call | tf_op jit(solution)/shard_map/pallas_call | solution.py:364

commit v2 on v1

--- a/solution.py
+++ b/solution.py
@@ -41,9 +41,9 @@
     n_kv,
     tok, gain, wq, wk, wv, qg, kg, wo, ch,
     out_ref, lt_ref,
-    x_buf, ch_s, ch_buf, raw_s, w_buf, wo_buf, g_buf, qg_buf, kg_buf,
+    x_buf, ch_s, ch_buf, raw_s, w_buf, wo_buf, g_buf, hg_buf,
     q_s, kv_all, kp_s, att_s, sum_s, part_send, part_recv,
-    load_sem, x_sem, send_sem, recv_sem, part_sem,
+    load_sem, x_sem, send_sem, stage_sem, end_sem, part_sem,
 ):
     me = lax.axis_index("kv")
     tp = lax.axis_index("tp")
@@ -67,30 +67,32 @@
     def span(start):
         return pl.ds(pl.multiple_of(start * half, LANES), half)
 
-    loads = {}
-
-    def load(name, src, dst):
-        copy = pltpu.make_async_copy(src, dst, load_sem.at[len(loads)])
-        copy.start()
-        loads[name] = copy
-
-    sides = ((0, tp), (1, partner))
-    load("tok", tok, x_buf.at[0])
-    load("g0", gain.at[:, span(tp)], g_buf.at[0])
-    for side, which in sides:
-        load(f"wk{side}", wk.at[span(which), :], w_buf.at[side, :, q_cols:q_cols + k_cols])
-        load(f"wv{side}", wv.at[span(which), :], w_buf.at[side, :, q_cols + k_cols:q_cols + 2 * k_cols])
-        load(f"wq{side}", wq.at[span(which), :], w_buf.at[side, :, 0:q_cols])
-    load("g1", gain.at[:, span(partner)], g_buf.at[1])
-    load("qg", qg, qg_buf)
-    load("kg", kg, kg_buf)
-    load("chs", ch, ch_s)
-    load("ch", ch, ch_buf)
-    for side, which in sides:
+    def load(sem, *pairs):
+        for src, dst in pairs:
+            pltpu.make_async_copy(src, dst, load_sem.at[sem]).start()
+
+    def loaded(sem, whole):
+        pltpu.make_async_copy(whole, whole, load_sem.at[sem]).wait()
+
+    def weights(side, which):
+        return (
+            (wk.at[span(which), :], w_buf.at[side, :, q_cols:q_cols + k_cols]),
+            (wv.at[span(which), :], w_buf.at[side, :, q_cols + k_cols:q_cols + 2 * k_cols]),
+            (wq.at[span(which), :], w_buf.at[side, :, 0:q_cols]),
+        )
+
+    TOK, GAIN, W0, W1, HEAD_GAIN, LIST, TABLE, OUT = range(8)
+    load(TOK, (tok, x_buf.at[0]))
+    load(GAIN, (gain.at[:, span(tp)], g_buf.at[0]), (gain.at[:, span(partner)], g_buf.at[1]))
+    load(W0, *weights(0, tp))
+    load(W1, *weights(1, partner))
+    load(HEAD_GAIN, (qg, hg_buf.at[0]), (kg, hg_buf.at[1]))
+    load(LIST, (ch, ch_s))
+    load(TABLE, (ch, ch_buf))
+    for side, which in ((0, tp), (1, partner)):
         for head in range(heads):
             to = head % group * LANES + head // group * HD
-            load(f"wo{side}{head}", wo.at[head * HD:(head + 1) * HD, span(which)],
-                 wo_buf.at[side, to:to + HD])
+            load(OUT, (wo.at[head * HD:(head + 1) * HD, span(which)], wo_buf.at[side, to:to + HD]))
 
     def device(row, col):
         return lax.rem(row + n_z, n_z) * N_Y + lax.rem(col + N_Y, N_Y)
@@ -108,15 +110,15 @@
         x = x_buf[side].astype(F32)
         return (x * g_buf[side]).astype(BF16), jnp.sum(x * x, axis=1, keepdims=True)
 
-    loads["tok"].wait()
+    loaded(TOK, x_buf.at[0])
     pl.semaphore_wait(barrier, 5)
     x_copy = pltpu.make_async_remote_copy(
         x_buf.at[0], x_buf.at[1], x_sem.at[0], x_sem.at[1],
         device_id={"tp": partner}, device_id_type=MESH)
     x_copy.start()
 
-    for name in ("g0", "wk0", "wv0", "wq0"):
-        loads[name].wait()
+    loaded(GAIN, g_buf)
+    loaded(W0, w_buf.at[0])
     y0, sq0 = scaled(0)
     raw_s[...] = dot(y0, w_buf[0])
 
@@ -130,10 +132,10 @@
         total = dot(hi, same_head) + dot(lo, same_head)
         return v * lax.rsqrt(total / HD + epsilon) * gain_row
 
-    for name in ("g1", "qg", "kg", "wk1", "wv1", "wq1"):
-        loads[name].wait()
-    qg_row = jnp.concatenate([qg_buf[...], qg_buf[...]], axis=1) * (HD ** -0.5 * LOG2E)
-    kg_row = jnp.concatenate([kg_buf[...], kg_buf[...]], axis=1)
+    loaded(HEAD_GAIN, hg_buf)
+    loaded(W1, w_buf.at[1])
+    qg_row = jnp.concatenate([hg_buf[0], hg_buf[0]], axis=1) * (HD ** -0.5 * LOG2E)
+    kg_row = jnp.concatenate([hg_buf[1], hg_buf[1]], axis=1)
     x_copy.wait()
     y1, sq1 = scaled(1)
     row_scale = lax.rsqrt((sq0 + sq1) / width + epsilon)
@@ -145,35 +147,47 @@
     kv_all[mine] = jnp.concatenate([key_part, value_part], axis=1).reshape(nb, BLK, 2 * k_cols)
 
     chunk_blocks = nb // CHUNKS
-    sent = []
-
-    def kv_copy(direction, owner, chunk):
-        at = pl.ds(1 + owner * nb + chunk * chunk_blocks, chunk_blocks)
+    sent = {UP: 0, DOWN: 0, LEFT: 0, RIGHT: 0}
+    most_sent = {UP: 0, DOWN: 0, LEFT: 0, RIGHT: 0}
+
+    def kv_copy(direction, row, col, chunk, arrival):
+        at = pl.ds(1 + (row * N_Y + col) * nb + chunk * chunk_blocks, chunk_blocks)
         return pltpu.make_async_remote_copy(
-            kv_all.at[at], kv_all.at[at],
-            send_sem.at[direction, chunk, owner], recv_sem.at[chunk, owner],
+            kv_all.at[at], kv_all.at[at], send_sem.at[direction], arrival,
             device_id={"kv": neighbour[direction]}, device_id_type=MESH)
 
-    def send(direction, owner, chunk, when):
-        sent.append((direction, owner, chunk, when))
+    def stage(kind, row, chunk):
+        return stage_sem.at[kind, row, chunk]
+
+    def send(direction, row, col, chunk, when, arrival):
+        if chunk == 0:
+            sent[direction] += jnp.where(when, 1, 0)
+            most_sent[direction] += 1
 
         @pl.when(when)
         def _():
-            kv_copy(direction, owner, chunk).start()
-
-    def arrive(owner, chunk, when):
+            kv_copy(direction, row, col, chunk, arrival).start()
+
+    def arrive(kind, row, col, chunk, when):
         @pl.when(when)
         def _():
-            kv_copy(UP, owner, chunk).wait_recv()
+            kv_copy(UP, row, col, chunk, stage(kind, row, chunk)).wait_recv()
+
+    def settle(count, most, sem):
+        for k in range(1, most + 1):
+            @pl.when(count == k)
+            def _():
+                whole = kv_all.at[0:k * nb]
+                pltpu.make_async_copy(whole, whole, sem).wait()
 
     last = n_z - 1
     reach_a, reach_b = n_z // 2, n_z // 2 - 1
     back_a, back_b = last - reach_a, last - reach_b
     for chunk in range(CHUNKS):
-        send(RIGHT, me, chunk, (z < last) | (y < N_Y - 1))
-        send(UP, me, chunk, z < last)
-        send(DOWN, me, chunk, z < back_a)
-        send(LEFT, me, chunk, y == 0)
+        send(RIGHT, z, y, chunk, (z < last) | (y < N_Y - 1), stage(1, z, chunk))
+        send(UP, z, y, chunk, z < last, stage(0, z, chunk))
+        send(DOWN, z, y, chunk, z < back_a, stage(0, z, chunk))
+        send(LEFT, z, y, chunk, y == 0, end_sem.at[0])
 
     raw = (raw_s[:, 0:q_cols] + dot(y1, w_buf[1, :, 0:q_cols])) * row_scale
     low = iota((rows, LANES), 1) < HD
@@ -188,8 +202,8 @@
             for r in range(nb):
                 q_s[r, head * BLK:(head + 1) * BLK] = here[r * BLK:(r + 1) * BLK]
 
-    loads["ch"].wait()
-    loads["chs"].wait()
+    loaded(TABLE, ch_buf)
+    loaded(LIST, ch_s)
     lists = ch_buf[...]
     lane = iota((nb, keys), 1)
     block = jnp.full((nb, keys), -1, jnp.int32)
@@ -199,38 +213,36 @@
     kp_s[...] = jnp.where(block < 0, 1 << 24, away).astype(F32)
 
     left_col = lax.rem(y + N_Y - 1, N_Y)
-    left_me = z * N_Y + left_col
     for chunk in range(CHUNKS):
-        arrive(left_me, chunk, (z < last) | (y > 0))
-        send(UP, left_me, chunk, z < last)
-        send(DOWN, left_me, chunk, z < back_b)
-        send(RIGHT, left_me, chunk, (y == 1) | (y == 2))
-
+        arrive(1, z, left_col, chunk, (z < last) | (y > 0))
+        send(UP, z, left_col, chunk, z < last, stage(1, z, chunk))
+        send(DOWN, z, left_col, chunk, z < back_b, stage(1, z, chunk))
+        send(RIGHT, z, left_col, chunk, (y == 1) | (y == 2), end_sem.at[1])
+
+    routes = (
+        (0, y, reach_a, back_a, LEFT, end_sem.at[0]),
+        (1, left_col, reach_b, back_b, RIGHT, end_sem.at[1]),
+    )
     for hop in range(1, n_z // 2 + 1):
-        above = z - hop
+        above = lax.max(z - hop, 0)
         below = lax.rem(z + hop, n_z)
-        for col, reach, back, side in ((y, reach_a, back_a, LEFT), (left_col, reach_b, back_b, RIGHT)):
+        for kind, col, reach, back, side, end in routes:
             for chunk in range(CHUNKS):
                 if hop <= reach:
-                    owner = lax.max(above, 0) * N_Y + col
-                    arrive(owner, chunk, above >= 0)
+                    valid = z >= hop
+                    arrive(kind, above, col, chunk, valid)
                     if hop < reach:
-                        send(UP, owner, chunk, (above >= 0) & (z < last))
-                    send(side, owner, chunk, above >= 0)
+                        send(UP, above, col, chunk, valid & (z < last), stage(kind, above, chunk))
+                    send(side, above, col, chunk, valid, end)
                 if hop <= back:
-                    owner = below * N_Y + col
                     valid = below < back
-                    arrive(owner, chunk, valid)
+                    arrive(kind, below, col, chunk, valid)
                     if hop < back:
-                        send(DOWN, owner, chunk, valid)
-                    send(side, owner, chunk, valid & (below < z))
-
-    right_col = lax.rem(y + 1, N_Y)
-    far_col = lax.rem(y + 2, N_Y)
-    for row in range(n_z):
-        for chunk in range(CHUNKS):
-            arrive(row * N_Y + right_col, chunk, (row < z) | ((row == z) & (y == N_Y - 1)))
-            arrive(row * N_Y + far_col, chunk, (row < z) | ((row == z) & (y >= 2)))
+                        send(DOWN, below, col, chunk, valid, stage(kind, below, chunk))
+                    send(side, below, col, chunk, valid & (below < z), end)
+
+    settle(z + jnp.where(y == N_Y - 1, 1, 0), n_z, end_sem.at[0])
+    settle(z + jnp.where(y >= 2, 1, 0), n_z, end_sem.at[1])
 
     query_row = iota((BLK, keys), 0).astype(F32)
     ones = jnp.ones((keys, LANES), BF16)
@@ -273,9 +285,7 @@
             sums = jnp.where(tile_lane == t + group, second[:, LANES:], sums)
         sum_s[at] = sums
 
-    for side in range(2):
-        for head in range(heads):
-            loads[f"wo{side}{head}"].wait()
+    loaded(OUT, wo_buf)
     part_rows = rows // PARTS
 
     def part_copy(part):
@@ -297,10 +307,8 @@
     logs = jnp.log(sum_s[...]) - slopes * alibi * row_in
     lt_ref[...] = logs.T[0:heads]
 
-    for direction, owner, chunk, when in sent:
-        @pl.when(when)
-        def _():
-            kv_copy(direction, owner, chunk).wait_send()
+    for direction in sent:
+        settle(sent[direction], most_sent[direction], send_sem.at[direction])
 
     for part in range(PARTS):
         at = slice(part * part_rows, (part + 1) * part_rows)
@@ -339,8 +347,7 @@
             vmem((2, half, q_cols + 2 * k_cols), BF16),
             vmem((2, q_cols, half), BF16),
             vmem((2, 1, half), F32),
-            vmem((1, HD), F32),
-            vmem((1, HD), F32),
+            vmem((2, 1, HD), F32),
             vmem((nb, heads * BLK, LANES), BF16),
             vmem((1 + n_kv * nb, BLK, 2 * k_cols), BF16),
             vmem((nb, entries * BLK), F32),
@@ -348,10 +355,11 @@
             vmem((rows, LANES), F32),
             vmem((rows, half), BF16),
             vmem((rows, half), BF16),
-            dma((13 + 2 * heads,)),
+            dma((8,)),
             dma((2,)),
-            dma((4, CHUNKS, n_kv)),
-            dma((CHUNKS, n_kv)),
+            dma((4,)),
+            dma((2, n_kv // N_Y, CHUNKS)),
+            dma((2,)),
             dma((2, PARTS)),
         ],
         compiler_params=pltpu.CompilerParams(

time: 41.6 us -> 38.9 us (0.935)
  Pallas kernels: 40.9 us -> 38.1 us
    pallas_call x1, Pallas kernels: 40.1 us -> 37.4 us  [shards(): pl.pallas_call(functools.partial(kernel, n_kv), out_shape=(vmem((rows, ha...]
where the time goes in v2:
time: 38.9 us; the launch traced here: 38.7 us
  Pallas kernels  38.1 us (98%)
  between operations  0.64 us (2%)
    pallas_call x1, Pallas kernels, shards(): pl.pallas_call(functools.partial(kernel, n_kv), out_shape=(vmem((rows, ha...  37.4 us

profile of v2, /device:TPU:193, one launch (start us, length us, event | category | flops | bytes accessed | tf_op | source)
XLA Modules:
  0.0 38.7 jit_solution(11891701956793365048)
XLA Ops:
  0.6 37.4 %shard_map.104 = (bf16[256,512]{1,0:T(8,128)(2,1)S(1)}, f32[8,256]{1,0:T(8,128)S(1)}) custom-call(bf16[256,512]{1,0:T(8,128)(2,1)} %bitcast.7, f32[1,1024]{1,0:T(1,128)} %bitcast.8, bf16[1024,512]{1,0:T(8,128)(2,1)} %wq.1, bf16[1024,128]{1,0:T(8,128)(2,1)} %wk.1, bf16[1024,128]{1,0:T(8,128)(2,1)} %wv.1, f32[1,64]{1,0:T(1,128)} %bitcast.10, ...), custom_call_target="tpu_custom_call" | custom-call | tf_op jit(solution)/shard_map/pallas_call | solution.py:337
  38.0 0.7 %shard_map.105 = (bf16[256,512]{1,0:T(8,128)(2,1)}, f32[8,256]{1,0:T(8,128)}) custom-call(bf16[256,512]{1,0:T(8,128)(2,1)S(1)} %get-tuple-element.6.mixed, f32[8,256]{1,0:T(8,128)S(1)} %get-tuple-element.7.log_total), custom_call_target="tpu_custom_call" | custom-call | tf_op jit(solution)/shard_map/pallas_call | solution.py:372

commit v3 on v2

v3 whole, which is shorter than its diff:
```python
import functools
import math

import jax
import jax.numpy as jnp
from jax import lax
from jax.experimental import pallas as pl
from jax.experimental.pallas import tpu as pltpu
from jax.sharding import PartitionSpec as P

HD = 64
BLK = 32
LANES = 128
MOST = 4
PARTS = 2
N_Y = 4
UP, DOWN, LEFT, RIGHT, FAR = range(5)

epsilon = 1e-06
alibi_reach = 4.0
LOG2E = math.log2(math.e)
F32 = jnp.float32
BF16 = jnp.bfloat16
NT = (((1,), (1,)), ((), ()))
MESH = pl.DeviceIdType.MESH


def iota(shape, dim):
    return lax.broadcasted_iota(jnp.int32, shape, dim)


def dot(a, b):
    return jnp.dot(a, b, preferred_element_type=F32)


def dot_nt(a, b):
    return lax.dot_general(a, b, NT, preferred_element_type=F32)


def kernel(
    n_kv,
    tok, gain, wq, wk, wv, qg, kg, wo, ch,
    out_ref, lt_ref,
    x_buf, ch_buf, raw_s, w_buf, wo_buf, g_buf, hg_buf,
    place_send, place_recv, code_s, index_v, index_s, left_s, right_s, far_s,
    q_s, kv, kp_s, att_s, sum_s, part_send, part_recv,
    load_sem, x_sem, place_sem, send_sem, stage_sem, end_sem, part_sem,
):
    me = lax.axis_index("kv")
    tp = lax.axis_index("tp")
    partner = 1 - tp
    n_z = n_kv // N_Y
    z = me // N_Y
    y = me % N_Y
    rows, half = tok.shape
    q_cols = wq.shape[1]
    k_cols = wk.shape[1]
    heads = q_cols // HD
    kv_heads = k_cols // HD
    group = heads // kv_heads
    n_heads = heads * lax.axis_size("tp")
    nb, entries = ch.shape
    n_blocks = n_kv * nb
    width = half * 2
    seq_len = rows * n_kv
    alibi = alibi_reach / seq_len
    keys = entries * BLK
    picked = MOST * BLK

    def span(start):
        return pl.ds(pl.multiple_of(start * half, LANES), half)

    def load(sem, *pairs):
        for src, dst in pairs:
            pltpu.make_async_copy(src, dst, load_sem.at[sem]).start()

    def loaded(sem, whole):
        pltpu.make_async_copy(whole, whole, load_sem.at[sem]).wait()

    def weights(side, which):
        return (
            (wk.at[span(which), :], w_buf.at[side, :, q_cols:q_cols + k_cols]),
            (wv.at[span(which), :], w_buf.at[side, :, q_cols + k_cols:q_cols + 2 * k_cols]),
            (wq.at[span(which), :], w_buf.at[side, :, 0:q_cols]),
        )

    TABLE, TOK, GAIN, W0, W1, HEAD_GAIN, OUT, INDEX = range(8)
    load(TABLE, (ch, ch_buf))
    load(TOK, (tok, x_buf.at[0]))
    load(GAIN, (gain.at[:, span(tp)], g_buf.at[0]), (gain.at[:, span(partner)], g_buf.at[1]))
    load(W0, *weights(0, tp))
    load(W1, *weights(1, partner))
    load(HEAD_GAIN, (qg, hg_buf.at[0]), (kg, hg_buf.at[1]))
    for side, which in ((0, tp), (1, partner)):
        for head in range(heads):
            to = head % group * LANES + head // group * HD
            load(OUT, (wo.at[head * HD:(head + 1) * HD, span(which)], wo_buf.at[side, to:to + HD]))

    def device(row, col):
        return lax.rem(row + n_z, n_z) * N_Y + lax.rem(col + N_Y, N_Y)

    neighbour = {
        UP: device(z + 1, y), DOWN: device(z - 1, y),
        LEFT: device(z, y - 1), RIGHT: device(z, y + 1), FAR: device(z, y + 2),
    }
    barrier = pltpu.get_barrier_semaphore()
    pl.semaphore_signal(barrier, inc=1, device_id={"tp": partner}, device_id_type=MESH)
    for target in neighbour.values():
        pl.semaphore_signal(barrier, inc=1, device_id={"kv": target}, device_id_type=MESH)

    loaded(TABLE, ch_buf)
    lists = ch_buf[...]
    lane_block = iota((nb, n_blocks), 1)
    hits = [lists[:, e:e + 1] == lane_block for e in range(entries)]
    hit = hits[0]
    for e in range(1, entries):
        hit = hit | hits[e]
    need = jnp.broadcast_to(jnp.max(jnp.where(hit, 1, 0), axis=0, keepdims=True), (nb, n_blocks))
    rank_of = jnp.zeros((nb, n_blocks), jnp.int32)
    for k in range(1, nb):
        rank_of = rank_of + jnp.where(lane_block % nb >= k, pltpu.roll(need, k, 1), 0)
    place_send[...] = jnp.where(need > 0, rank_of, -1).astype(F32)

    def scaled(side):
        x = x_buf[side].astype(F32)
        return (x * g_buf[side]).astype(BF16), jnp.sum(x * x, axis=1, keepdims=True)

    loaded(TOK, x_buf.at[0])
    pl.semaphore_wait(barrier, 1 + len(neighbour))
    x_copy = pltpu.make_async_remote_copy(
        x_buf.at[0], x_buf.at[1], x_sem.at[0], x_sem.at[1],
        device_id={"tp": partner}, device_id_type=MESH)
    x_copy.start()

    def place_copy(direction, slot):
        return pltpu.make_async_remote_copy(
            place_send, place_recv.at[slot], place_sem.at[0, slot], place_sem.at[1, slot],
            device_id={"kv": neighbour[direction]}, device_id_type=MESH)

    place_copies = [place_copy(RIGHT, 0), place_copy(LEFT, 1), place_copy(FAR, 2)]
    for copy in place_copies:
        copy.start()

    loaded(GAIN, g_buf)
    loaded(W0, w_buf.at[0])
    y0, sq0 = scaled(0)
    raw_s[...] = dot(y0, w_buf[0])

    same_head = jnp.where(
        iota((LANES, LANES), 0) // HD == iota((LANES, LANES), 1) // HD, 1.0, 0.0).astype(BF16)

    def head_norm(v, gain_row):
        sq = v * v
        hi = sq.astype(BF16)
        lo = (sq - hi.astype(F32)).astype(BF16)
        total = dot(hi, same_head) + dot(lo, same_head)
        return v * lax.rsqrt(total / HD + epsilon) * gain_row

    loaded(HEAD_GAIN, hg_buf)
    loaded(W1, w_buf.at[1])
    qg_row = jnp.concatenate([hg_buf[0], hg_buf[0]], axis=1) * (HD ** -0.5 * LOG2E)
    kg_row = jnp.concatenate([hg_buf[1], hg_buf[1]], axis=1)
    low = iota((rows, LANES), 1) < HD
    x_copy.wait()
    y1, sq1 = scaled(1)
    row_scale = lax.rsqrt((sq0 + sq1) / width + epsilon)
    raw_kv = (raw_s[:, q_cols:] + dot(y1, w_buf[1, :, q_cols:])) * row_scale
    key_part = pltpu.roll(head_norm(raw_kv[:, 0:k_cols], kg_row), HD, 1)
    value_part = raw_kv[:, k_cols:]

    def base(row, col):
        return 1 + (row * N_Y + col) * nb

    own_tiles = (jnp.where(low, value_part, key_part), jnp.where(low, key_part, value_part))
    for tile in range(2):
        kv[tile, 0] = jnp.zeros((BLK, LANES), BF16)
        kv[tile, pl.ds(base(z, y), nb)] = own_tiles[tile].astype(BF16).reshape(nb, BLK, LANES)

    last = n_z - 1
    reach_a, reach_b = n_z // 2, n_z // 2 - 1
    back_a, back_b = last - reach_a, last - reach_b
    sent = []

    def send(direction, src, dst, units, arrival, when, hop=None):
        sent.append((units, when, hop is not None))

        @pl.when(when(z, y, hop))
        def _():
            pltpu.make_async_remote_copy(
                src, dst, send_sem.at[0], arrival,
                device_id={"kv": neighbour[direction]}, device_id_type=MESH).start()

    def stage(kind, row):
        return stage_sem.at[kind, row]

    def tile_of(kind):
        return kind % 2

    def whole(kind, row, col):
        return kv.at[tile_of(kind), pl.ds(base(row, col), nb)]

    def send_whole(direction, kind, row, col, when, hop=None):
        part = whole(kind, row, col)
        send(direction, part, part, 2, stage(kind, row), when, hop)

    def arrive(kind, row, col, when, hop=None):
        @pl.when(when(z, y, hop))
        def _():
            part = whole(kind, row, col)
            pltpu.make_async_remote_copy(
                part, part, send_sem.at[0], stage(kind, row),
                device_id={"kv": neighbour[UP]}, device_id_type=MESH).wait_recv()

    same_row = iota((picked, rows), 0) % BLK == iota((picked, rows), 1) % BLK
    row_slot = (iota((picked, rows), 0) // BLK).astype(F32)

    def chooser(which, row):
        code = code_s[which, pl.ds(row, 1), :]
        return jnp.where(same_row & (code == row_slot), 1.0, 0.0).astype(BF16)

    def item(kind, row, col):
        return kv[tile_of(kind), pl.ds(base(row, col), nb)].reshape(rows, LANES)

    def blocks(x):
        return x.astype(BF16).reshape(-1, BLK, LANES)

    def choose_a(row, to_left, to_right, to_far, hop=None):
        @pl.when(to_left(z, y, hop) | to_right(z, y, hop) | to_far(z, y, hop))
        def _():
            left, right, far = (chooser(i, row) for i in range(3))
            left_s[row, 0] = blocks(dot(left, item(0, row, y)))
            found = blocks(dot(jnp.concatenate([left, right, far], axis=0), item(1, row, y)))
            left_s[row, 1] = found[0:MOST]
            right_s[row, 0] = found[MOST:2 * MOST]
            far_s[row] = found[2 * MOST:]

        at = pl.ds(base(row, y), MOST)
        send(LEFT, left_s.at[row], kv.at[:, at], 2, end_sem.at[0], to_left, hop)
        send(RIGHT, right_s.at[row, 0], kv.at[1, at], 1, end_sem.at[0], to_right, hop)
        send(FAR, far_s.at[row], kv.at[1, at], 1, end_sem.at[0], to_far, hop)

    def choose_b(row, to_right, hop=None):
        @pl.when(to_right(z, y, hop))
        def _():
            right_s[row, 1] = blocks(dot(chooser(3, row), item(2, row, left_col)))

        at = pl.ds(base(row, left_col), MOST)
        send(RIGHT, right_s.at[row, 1], kv.at[0, at], 1, end_sem.at[0], to_right, hop)

    left_col = lax.rem(y + N_Y - 1, N_Y)
    send_whole(UP, 0, z, y, lambda z, y, hop: z < last)
    send_whole(DOWN, 0, z, y, lambda z, y, hop: z < back_a)
    send(RIGHT, whole(0, z, y), whole(0, z, y), 2, stage(2, z), lambda z, y, hop: (z < last) | (y < N_Y - 1))
    send_whole(UP, 1, z, y, lambda z, y, hop: z < last)
    send_whole(DOWN, 1, z, y, lambda z, y, hop: z < back_a)

    raw = (raw_s[:, 0:q_cols] + dot(y1, w_buf[1, :, 0:q_cols])) * row_scale
    for tile in range(q_cols // LANES):
        q = head_norm(raw[:, tile * LANES:(tile + 1) * LANES], qg_row)
        turned = pltpu.roll(q, HD, 1)
        for odd in range(2):
            head = 2 * tile + odd
            side = head // group
            here = turned if odd == side else q
            here = jnp.where(low if side == 1 else ~low, here, 0.0).astype(BF16)
            for r in range(nb):
                q_s[r, head * BLK:(head + 1) * BLK] = here[r * BLK:(r + 1) * BLK]

    arrive(2, z, left_col, lambda z, y, hop: (z < last) | (y > 0))
    send_whole(UP, 2, z, left_col, lambda z, y, hop: z < last)
    send_whole(DOWN, 2, z, left_col, lambda z, y, hop: z < back_b)

    for copy in place_copies:
        copy.wait()
    spread = jnp.where(
        iota((n_blocks, rows), 0) % nb == iota((n_blocks, rows), 1) // BLK, 1.0, 0.0).astype(BF16)
    row_owner = iota((n_z, n_blocks), 0) * N_Y
    owner_lane = iota((n_z, n_blocks), 1) // nb
    for which, (slot, col) in enumerate(((0, y), (1, y), (2, y), (1, left_col))):
        mine = jnp.where(owner_lane == row_owner + col, place_recv[slot], 0.0)
        code_s[which] = dot(mine.astype(BF16), spread)

    lane_entry = iota((nb, entries), 1)
    rank = jnp.zeros((nb, entries), jnp.int32)
    for e in range(entries):
        found = jnp.max(jnp.where(hits[e], rank_of, 0), axis=1, keepdims=True)
        rank = jnp.where(lane_entry == e, found, rank)
    owner = lists // nb
    col = lax.rem(owner, N_Y)
    ranked = 1 + owner * nb + rank
    for tile in range(2):
        full = col == y
        if tile == 0:
            full = full | (col == left_col)
        index_v[tile] = jnp.where(lists < 0, 0, jnp.where(full, 1 + lists, ranked))
    index_copy = pltpu.make_async_copy(index_v, index_s, load_sem.at[INDEX])
    index_copy.start()

    lane = iota((nb, keys), 1)
    block = jnp.full((nb, keys), -1, jnp.int32)
    for e in range(entries):
        block = jnp.where(lane // BLK == e, lists[:, e:e + 1], block)
    away = (block - (me * nb + iota((nb, keys), 0))) * BLK + lane % BLK
    kp_s[...] = jnp.where(block < 0, 1 << 24, away).astype(F32)

    choose_a(z, lambda z, y, hop: y == 0, lambda z, y, hop: y < N_Y - 1, lambda z, y, hop: y < N_Y - 2)
    choose_b(z, lambda z, y, hop: (y == 1) | (y == 2))

    routes = (((0, 1), y, reach_a, back_a), ((2,), left_col, reach_b, back_b))
    hops = range(1, n_z // 2 + 1)

    def one_hop(hop, carry):
        above = lax.max(z - hop, 0)
        below = lax.rem(z + hop, n_z)
        for kinds, col, reach, back in routes:

            def from_above(z, y, hop, reach=reach):
                return (z >= hop) & (hop <= reach)

            def go_up(z, y, hop, reach=reach):
                return (z >= hop) & (hop < reach) & (z < last)

            def from_below(z, y, hop, back=back):
                return ((z + hop) % n_z < back) & (hop <= back)

            def go_down(z, y, hop, back=back):
                return ((z + hop) % n_z < back) & (hop < back)

            def use_below(z, y, hop, back=back):
                return ((z + hop) % n_z < back) & (hop <= back) & ((z + hop) % n_z < z)

            for kind in kinds:
                arrive(kind, above, col, from_above, hop)
                send_whole(UP, kind, above, col, go_up, hop)
                arrive(kind, below, col, from_below, hop)
                send_whole(DOWN, kind, below, col, go_down, hop)
            for row, use in ((above, from_above), (below, use_below)):
                if len(kinds) == 2:
                    choose_a(row, use, use, use, hop)
                else:
                    choose_b(row, use, hop)
        return carry

    lax.fori_loop(hops.start, hops.stop, one_hop, 0)

    def settle(count, sem):
        for k in range(n_z):
            @pl.when(z == k)
            def _():
                for j in range(N_Y):
                    units = count(k, j)
                    if units:
                        @pl.when(y == j)
                        def _():
                            part = kv.at[:, 0:units * MOST // 2]
                            pltpu.make_async_copy(part, part, sem).wait()

    settle(lambda z, y: 2 * (z + (y == N_Y - 1)) + (z + (y >= 1)) + 2 * (z + (y >= 2)), end_sem.at[0])
    index_copy.wait()

    query_row = iota((BLK, keys), 0).astype(F32)
    ones = jnp.ones((keys, LANES), BF16)
    tile_low = iota((BLK, LANES), 1) < HD
    tile_lane = iota((BLK, LANES), 1)
    core_slope = jnp.where(tp == 0, 1.0, 2.0 ** (-8.0 * heads / n_heads)).astype(F32)

    def slope_of(head):
        return core_slope * (2.0 ** (-8.0 * (head + 1) / n_heads))

    def attend(r):
        key_pos = kp_s[pl.ds(r, 1), :]
        allowed = key_pos <= query_row
        outs = []
        for side in range(kv_heads):
            both = jnp.concatenate([kv[side, index_s[side, r, e]] for e in range(entries)], axis=0)
            scores = dot_nt(q_s[r, side * group * BLK:(side + 1) * group * BLK], both)
            weights = []
            for t in range(group):
                bias = key_pos * (slope_of(side * group + t) * (alibi * LOG2E))
                part = jnp.exp2(scores[t * BLK:(t + 1) * BLK] + bias)
                weights.append(jnp.where(allowed, part, 0.0).astype(BF16))
            outs.append(dot(jnp.concatenate(weights, axis=0), jnp.concatenate([both, ones], axis=1)))

        sums = jnp.ones((BLK, LANES), F32)
        at = pl.ds(pl.multiple_of(r * BLK, BLK), BLK)
        for t in range(group):
            first, second = (o[t * BLK:(t + 1) * BLK] for o in outs)
            top = jnp.where(tile_low, first[:, 0:LANES], second[:, 0:LANES])
            total = jnp.where(tile_low, first[:, LANES:], second[:, LANES:])
            att_s[at, t * LANES:(t + 1) * LANES] = (top / total).astype(BF16)
            sums = jnp.where(tile_lane == t, first[:, LANES:], sums)
            sums = jnp.where(tile_lane == t + group, second[:, LANES:], sums)
        sum_s[at] = sums

    loaded(OUT, wo_buf)
    part_rows = rows // PARTS

    def part_at(part):
        return pl.ds(pl.multiple_of(part * part_rows, part_rows), part_rows)

    def part_copy(part):
        at = part_at(part)
        return pltpu.make_async_remote_copy(
            part_send.at[at], part_recv.at[at], part_sem.at[0, part], part_sem.at[1, part],
            device_id={"tp": partner}, device_id_type=MESH)

    def one_part(part, carry):
        for r in range(nb // PARTS):
            attend(part * (nb // PARTS) + r)
        at = part_at(part)
        part_send[at] = dot(att_s[at], wo_buf[1]).astype(BF16)
        part_copy(part).start()
        return carry

    lax.fori_loop(0, PARTS, one_part, 0)

    own = dot(att_s[...], wo_buf[0])
    row_in = (iota((rows, LANES), 0) % BLK).astype(F32)
    slopes = jnp.exp2(-8.0 / n_heads * (tp * heads + iota((rows, LANES), 1) + 1).astype(F32))
    logs = jnp.log(sum_s[...]) - slopes * alibi * row_in
    lt_ref[...] = logs.T[0:heads]

    def all_sent(z, y):
        return sum(
            units for units, when, looped in sent
            for hop in (hops if looped else (0,)) if when(z, y, hop))

    settle(all_sent, send_sem.at[0])

    for part in range(PARTS):
        at = slice(part * part_rows, (part + 1) * part_rows)
        part_copy(part).wait()
        out_ref[at] = (own[at] + part_recv[at].astype(F32)).astype(BF16)


def write_out(mixed, log_total, mixed_out, log_out, sems):
    copies = [
        pltpu.make_async_copy(mixed, mixed_out, sems.at[0]),
        pltpu.make_async_copy(log_total, log_out, sems.at[1]),
    ]
    for copy in copies:
        copy.start()
    for copy in copies:
        copy.wait()


def shards(n_kv, tokens, norm_gain, w_query, w_key, w_value, q_gain, k_gain, w_out, chosen):
    seqs, rows, half = tokens.shape
    nb, entries = chosen.shape[1:]
    q_cols, k_cols = w_query.shape[1], w_key.shape[1]
    heads = q_cols // HD
    n_z = n_kv // N_Y
    vmem = pltpu.VMEM
    dma = pltpu.SemaphoreType.DMA
    mixed, log_total = pl.pallas_call(
        functools.partial(kernel, n_kv),
        out_shape=(vmem((rows, half), BF16), vmem((heads, rows), F32)),
        in_specs=[pl.BlockSpec(memory_space=pltpu.HBM)] * 9,
        out_specs=(pl.BlockSpec(memory_space=vmem), pl.BlockSpec(memory_space=vmem)),
        scratch_shapes=[
            vmem((2, rows, half), BF16),
            vmem((nb, entries), jnp.int32),
            vmem((rows, q_cols + 2 * k_cols), F32),
            vmem((2, half, q_cols + 2 * k_cols), BF16),
            vmem((2, q_cols, half), BF16),
            vmem((2, 1, half), F32),
            vmem((2, 1, HD), F32),
            vmem((nb, n_kv * nb), F32),
            vmem((3, nb, n_kv * nb), F32),
            vmem((4, n_z, rows), F32),
            vmem((2, nb, entries), jnp.int32),
            pltpu.SMEM((2, nb, entries), jnp.int32),
            vmem((n_z, 2, MOST, BLK, LANES), BF16),
            vmem((n_z, 2, MOST, BLK, LANES), BF16),
            vmem((n_z, MOST, BLK, LANES), BF16),
            vmem((nb, heads * BLK, LANES), BF16),
            vmem((2, 1 + n_kv * nb, BLK, LANES), BF16),
            vmem((nb, entries * BLK), F32),
            vmem((rows, q_cols), BF16),
            vmem((rows, LANES), F32),
            vmem((rows, half), BF16),
            vmem((rows, half), BF16),
            dma((8,)),
            dma((2,)),
            dma((2, 3)),
            dma((1,)),
            dma((3, n_z)),
            dma((1,)),
            dma((2, PARTS)),
        ],
        compiler_params=pltpu.CompilerParams(
            collective_id=0, has_side_effects=True, vmem_limit_bytes=66_700_000
        ),
    )(
        tokens.reshape(rows, half), norm_gain.reshape(1, -1), w_query, w_key, w_value,
        q_gain.reshape(1, -1), k_gain.reshape(1, -1), w_out, chosen.reshape(nb, entries),
    )
    mixed, log_total = pl.pallas_call(
        write_out,
        out_shape=(
            jax.ShapeDtypeStruct((rows, half), BF16),
            jax.ShapeDtypeStruct((heads, rows), F32),
        ),
        in_specs=[pl.BlockSpec(memory_space=pl.ANY)] * 2,
        out_specs=(pl.BlockSpec(memory_space=pltpu.HBM),) * 2,
        scratch_shapes=[dma((2,))],
        compiler_params=pltpu.CompilerParams(vmem_limit_bytes=1_000_000),
    )(mixed, log_total)
    return mixed.reshape(seqs, rows, half), log_total.reshape(seqs, heads, rows)


def solution(mesh):
    in_specs = (
        P("dp", "kv", "tp"),
        P(),
        P(None, "tp"),
        P(None, "tp"),
        P(None, "tp"),
        P(),
        P(),
        P("tp", None),
        P("dp", "kv", None),
    )
    out_specs = (P("dp", "kv", "tp"), P("dp", "tp", "kv"))
    return jax.shard_map(
        functools.partial(shards, mesh.shape["kv"]),
        mesh=mesh, in_specs=in_specs, out_specs=out_specs, check_vma=False)
```

time: 38.9 us -> 33.5 us (0.86)
  Pallas kernels: 38.1 us -> 32.8 us
    pallas_call x1, Pallas kernels: 37.4 us -> 32.1 us  [shards(): pl.pallas_call(functools.partial(kernel, n_kv), out_shape=(vmem((rows, ha...]
where the time goes in v3:
time: 33.5 us; the launch traced here: 33.4 us
  Pallas kernels  32.8 us (98%)
  between operations  0.64 us (2%)
    pallas_call x1, Pallas kernels, shards(): pl.pallas_call(functools.partial(kernel, n_kv), out_shape=(vmem((rows, ha...  32.1 us
    pallas_call x1, Pallas kernels, shards(): pl.pallas_call(write_out, out_shape=(jax.ShapeDtypeStruct((rows, half), B...  0.72 us

profile of v3, /device:TPU:193, one launch (start us, length us, event | category | flops | bytes accessed | tf_op | source)
XLA Modules:
  0.0 33.4 jit_solution(3715810415653418207)
XLA Ops:
  0.6 32.1 %shard_map.104 = (bf16[256,512]{1,0:T(8,128)(2,1)S(1)}, f32[8,256]{1,0:T(8,128)S(1)}) custom-call(bf16[256,512]{1,0:T(8,128)(2,1)} %bitcast.7, f32[1,1024]{1,0:T(1,128)} %bitcast.8, bf16[1024,512]{1,0:T(8,128)(2,1)} %wq.1, bf16[1024,128]{1,0:T(8,128)(2,1)} %wk.1, bf16[1024,128]{1,0:T(8,128)(2,1)} %wv.1, f32[1,64]{1,0:T(1,128)} %bitcast.10, ...), custom_call_target="tpu_custom_call" | custom-call | tf_op jit(solution)/shard_map/pallas_call | solution.py:455
  32.7 0.7 %shard_map.105 = (bf16[256,512]{1,0:T(8,128)(2,1)}, f32[8,256]{1,0:T(8,128)}) custom-call(bf16[256,512]{1,0:T(8,128)(2,1)S(1)} %get-tuple-element.6.mixed, f32[8,256]{1,0:T(8,128)S(1)} %get-tuple-element.7.log_total), custom_call_target="tpu_custom_call" | custom-call | tf_op jit(solution)/shard_map/pallas_call | solution.py:498

commit v4 on v3

--- a/solution.py
+++ b/solution.py
@@ -43,7 +43,7 @@
     out_ref, lt_ref,
     x_buf, ch_buf, raw_s, w_buf, wo_buf, g_buf, hg_buf,
     place_send, place_recv, code_s, index_v, index_s, left_s, right_s, far_s,
-    q_s, kv, kp_s, att_s, sum_s, part_send, part_recv,
+    q_s, kv0, kv1, kp_s, found_s, att_s, sum_s, part_send, part_recv,
     load_sem, x_sem, place_sem, send_sem, stage_sem, end_sem, part_sem,
 ):
     me = lax.axis_index("kv")
@@ -66,35 +66,7 @@
     alibi = alibi_reach / seq_len
     keys = entries * BLK
     picked = MOST * BLK
-
-    def span(start):
-        return pl.ds(pl.multiple_of(start * half, LANES), half)
-
-    def load(sem, *pairs):
-        for src, dst in pairs:
-            pltpu.make_async_copy(src, dst, load_sem.at[sem]).start()
-
-    def loaded(sem, whole):
-        pltpu.make_async_copy(whole, whole, load_sem.at[sem]).wait()
-
-    def weights(side, which):
-        return (
-            (wk.at[span(which), :], w_buf.at[side, :, q_cols:q_cols + k_cols]),
-            (wv.at[span(which), :], w_buf.at[side, :, q_cols + k_cols:q_cols + 2 * k_cols]),
-            (wq.at[span(which), :], w_buf.at[side, :, 0:q_cols]),
-        )
-
-    TABLE, TOK, GAIN, W0, W1, HEAD_GAIN, OUT, INDEX = range(8)
-    load(TABLE, (ch, ch_buf))
-    load(TOK, (tok, x_buf.at[0]))
-    load(GAIN, (gain.at[:, span(tp)], g_buf.at[0]), (gain.at[:, span(partner)], g_buf.at[1]))
-    load(W0, *weights(0, tp))
-    load(W1, *weights(1, partner))
-    load(HEAD_GAIN, (qg, hg_buf.at[0]), (kg, hg_buf.at[1]))
-    for side, which in ((0, tp), (1, partner)):
-        for head in range(heads):
-            to = head % group * LANES + head // group * HD
-            load(OUT, (wo.at[head * HD:(head + 1) * HD, span(which)], wo_buf.at[side, to:to + HD]))
+    kv = (kv0, kv1)
 
     def device(row, col):
         return lax.rem(row + n_z, n_z) * N_Y + lax.rem(col + N_Y, N_Y)
@@ -107,6 +79,42 @@
     pl.semaphore_signal(barrier, inc=1, device_id={"tp": partner}, device_id_type=MESH)
     for target in neighbour.values():
         pl.semaphore_signal(barrier, inc=1, device_id={"kv": target}, device_id_type=MESH)
+
+    def span(start):
+        return pl.ds(pl.multiple_of(start * half, LANES), half)
+
+    def load(sem, *pairs):
+        for src, dst in pairs:
+            pltpu.make_async_copy(src, dst, load_sem.at[sem]).start()
+
+    def loaded(sem, whole):
+        pltpu.make_async_copy(whole, whole, load_sem.at[sem]).wait()
+
+    def weights(side, which):
+        return (
+            (wk.at[span(which), :], w_buf.at[side, :, q_cols:q_cols + k_cols]),
+            (wv.at[span(which), :], w_buf.at[side, :, q_cols + k_cols:q_cols + 2 * k_cols]),
+            (wq.at[span(which), :], w_buf.at[side, :, 0:q_cols]),
+        )
+
+    TABLE, TOK, GAIN, W0, W1, HEAD_GAIN, OUT, INDEX = range(8)
+    load(TOK, (tok, x_buf.at[0]))
+    load(TABLE, (ch, ch_buf))
+    load(GAIN, (gain.at[:, span(tp)], g_buf.at[0]), (gain.at[:, span(partner)], g_buf.at[1]))
+    load(W0, *weights(0, tp))
+    load(W1, *weights(1, partner))
+    load(HEAD_GAIN, (qg, hg_buf.at[0]), (kg, hg_buf.at[1]))
+
+    def scaled(side):
+        x = x_buf[side].astype(F32)
+        return (x * g_buf[side]).astype(BF16), jnp.sum(x * x, axis=1, keepdims=True)
+
+    loaded(TOK, x_buf.at[0])
+    pl.semaphore_wait(barrier, 1 + len(neighbour))
+    x_copy = pltpu.make_async_remote_copy(
+        x_buf.at[0], x_buf.at[1], x_sem.at[0], x_sem.at[1],
+        device_id={"tp": partner}, device_id_type=MESH)
+    x_copy.start()
 
     loaded(TABLE, ch_buf)
     lists = ch_buf[...]
@@ -121,17 +129,6 @@
         rank_of = rank_of + jnp.where(lane_block % nb >= k, pltpu.roll(need, k, 1), 0)
     place_send[...] = jnp.where(need > 0, rank_of, -1).astype(F32)
 
-    def scaled(side):
-        x = x_buf[side].astype(F32)
-        return (x * g_buf[side]).astype(BF16), jnp.sum(x * x, axis=1, keepdims=True)
-
-    loaded(TOK, x_buf.at[0])
-    pl.semaphore_wait(barrier, 1 + len(neighbour))
-    x_copy = pltpu.make_async_remote_copy(
-        x_buf.at[0], x_buf.at[1], x_sem.at[0], x_sem.at[1],
-        device_id={"tp": partner}, device_id_type=MESH)
-    x_copy.start()
-
     def place_copy(direction, slot):
         return pltpu.make_async_remote_copy(
             place_send, place_recv.at[slot], place_sem.at[0, slot], place_sem.at[1, slot],
@@ -140,6 +137,11 @@
     place_copies = [place_copy(RIGHT, 0), place_copy(LEFT, 1), place_copy(FAR, 2)]
     for copy in place_copies:
         copy.start()
+
+    for side, which in ((0, tp), (1, partner)):
+        for head in range(heads):
+            to = head % group * LANES + head // group * HD
+            load(OUT, (wo.at[head * HD:(head + 1) * HD, span(which)], wo_buf.at[side, to:to + HD]))
 
     loaded(GAIN, g_buf)
     loaded(W0, w_buf.at[0])
@@ -173,8 +175,8 @@
 
     own_tiles = (jnp.where(low, value_part, key_part), jnp.where(low, key_part, value_part))
     for tile in range(2):
-        kv[tile, 0] = jnp.zeros((BLK, LANES), BF16)
-        kv[tile, pl.ds(base(z, y), nb)] = own_tiles[tile].astype(BF16).reshape(nb, BLK, LANES)
+        kv[tile][0] = jnp.zeros((BLK, LANES), BF16)
+        kv[tile][pl.ds(base(z, y), nb)] = own_tiles[tile].astype(BF16).reshape(nb, BLK, LANES)
 
     last = n_z - 1
     reach_a, reach_b = n_z // 2, n_z // 2 - 1
@@ -182,12 +184,13 @@
     sent = []
 
     def send(direction, src, dst, units, arrival, when, hop=None):
+        chain = 0 if units == 2 else 1
         sent.append((units, when, hop is not None))
 
         @pl.when(when(z, y, hop))
         def _():
             pltpu.make_async_remote_copy(
-                src, dst, send_sem.at[0], arrival,
+                src, dst, send_sem.at[chain], arrival,
                 device_id={"kv": neighbour[direction]}, device_id_type=MESH).start()
 
     def stage(kind, row):
@@ -197,7 +200,7 @@
         return kind % 2
 
     def whole(kind, row, col):
-        return kv.at[tile_of(kind), pl.ds(base(row, col), nb)]
+        return kv[tile_of(kind)].at[pl.ds(base(row, col), nb)]
 
     def send_whole(direction, kind, row, col, when, hop=None):
         part = whole(kind, row, col)
@@ -219,40 +222,57 @@
         return jnp.where(same_row & (code == row_slot), 1.0, 0.0).astype(BF16)
 
     def item(kind, row, col):
-        return kv[tile_of(kind), pl.ds(base(row, col), nb)].reshape(rows, LANES)
+        return kv[tile_of(kind)][pl.ds(base(row, col), nb)].reshape(rows, LANES)
 
     def blocks(x):
         return x.astype(BF16).reshape(-1, BLK, LANES)
 
-    def choose_a(row, to_left, to_right, to_far, hop=None):
+    def send_chosen(direction, buf, tile, row, col, when, hop=None):
+        send(direction, buf, kv[tile].at[pl.ds(base(row, col), MOST)], 1, end_sem.at[tile], when, hop)
+
+    def choose_1(row, to_left, to_right, to_far, hop=None):
         @pl.when(to_left(z, y, hop) | to_right(z, y, hop) | to_far(z, y, hop))
         def _():
-            left, right, far = (chooser(i, row) for i in range(3))
-            left_s[row, 0] = blocks(dot(left, item(0, row, y)))
-            found = blocks(dot(jnp.concatenate([left, right, far], axis=0), item(1, row, y)))
-            left_s[row, 1] = found[0:MOST]
-            right_s[row, 0] = found[MOST:2 * MOST]
-            far_s[row] = found[2 * MOST:]
-
-        at = pl.ds(base(row, y), MOST)
-        send(LEFT, left_s.at[row], kv.at[:, at], 2, end_sem.at[0], to_left, hop)
-        send(RIGHT, right_s.at[row, 0], kv.at[1, at], 1, end_sem.at[0], to_right, hop)
-        send(FAR, far_s.at[row], kv.at[1, at], 1, end_sem.at[0], to_far, hop)
-
-    def choose_b(row, to_right, hop=None):
+            code = jnp.concatenate([chooser(i, row) for i in (2, 0, 1)], axis=0)
+            found = blocks(dot(code, item(1, row, y)))
+            far_s[row, 1] = found[0:MOST]
+            left_s[row, 1] = found[MOST:2 * MOST]
+            right_s[row, 1] = found[2 * MOST:]
+
+        send_chosen(FAR, far_s.at[row, 1], 1, row, y, to_far, hop)
+        send_chosen(LEFT, left_s.at[row, 1], 1, row, y, to_left, hop)
+        send_chosen(RIGHT, right_s.at[row, 1], 1, row, y, to_right, hop)
+
+    def choose_0(row, to_left, hop=None):
+        @pl.when(to_left(z, y, hop))
+        def _():
+            left_s[row, 0] = blocks(dot(chooser(0, row), item(0, row, y)))
+
+        send_chosen(LEFT, left_s.at[row, 0], 0, row, y, to_left, hop)
+
+    def choose_2(row, to_right, hop=None):
         @pl.when(to_right(z, y, hop))
         def _():
-            right_s[row, 1] = blocks(dot(chooser(3, row), item(2, row, left_col)))
-
-        at = pl.ds(base(row, left_col), MOST)
-        send(RIGHT, right_s.at[row, 1], kv.at[0, at], 1, end_sem.at[0], to_right, hop)
+            right_s[row, 0] = blocks(dot(chooser(3, row), item(2, row, left_col)))
+
+        send_chosen(RIGHT, right_s.at[row, 0], 0, row, left_col, to_right, hop)
+
+    def choose_last(to_right, to_far):
+        @pl.when(to_right(z, y, None))
+        def _():
+            code = jnp.concatenate([chooser(i, z) for i in (2, 1)], axis=0)
+            found = blocks(dot(code, item(0, z, y)))
+            far_s[z, 0] = found[0:MOST]
+            right_s[z, 0] = found[MOST:]
+
+        send_chosen(FAR, far_s.at[z, 0], 0, z, y, to_far)
+        send_chosen(RIGHT, right_s.at[z, 0], 0, z, y, to_right)
 
     left_col = lax.rem(y + N_Y - 1, N_Y)
-    send_whole(UP, 0, z, y, lambda z, y, hop: z < last)
-    send_whole(DOWN, 0, z, y, lambda z, y, hop: z < back_a)
-    send(RIGHT, whole(0, z, y), whole(0, z, y), 2, stage(2, z), lambda z, y, hop: (z < last) | (y < N_Y - 1))
-    send_whole(UP, 1, z, y, lambda z, y, hop: z < last)
-    send_whole(DOWN, 1, z, y, lambda z, y, hop: z < back_a)
+    send(RIGHT, whole(0, z, y), whole(0, z, y), 2, stage(2, z), lambda z, y, hop: z < last)
+    for kind in (1, 0):
+        send_whole(UP, kind, z, y, lambda z, y, hop: z < last)
+        send_whole(DOWN, kind, z, y, lambda z, y, hop: z < back_a)
 
     raw = (raw_s[:, 0:q_cols] + dot(y1, w_buf[1, :, 0:q_cols])) * row_scale
     for tile in range(q_cols // LANES):
@@ -266,7 +286,7 @@
             for r in range(nb):
                 q_s[r, head * BLK:(head + 1) * BLK] = here[r * BLK:(r + 1) * BLK]
 
-    arrive(2, z, left_col, lambda z, y, hop: (z < last) | (y > 0))
+    arrive(2, z, left_col, lambda z, y, hop: z < last)
     send_whole(UP, 2, z, left_col, lambda z, y, hop: z < last)
     send_whole(DOWN, 2, z, left_col, lambda z, y, hop: z < back_b)
 
@@ -286,12 +306,13 @@
         found = jnp.max(jnp.where(hits[e], rank_of, 0), axis=1, keepdims=True)
         rank = jnp.where(lane_entry == e, found, rank)
     owner = lists // nb
+    owner_row = owner // N_Y
     col = lax.rem(owner, N_Y)
     ranked = 1 + owner * nb + rank
     for tile in range(2):
         full = col == y
         if tile == 0:
-            full = full | (col == left_col)
+            full = full | ((col == left_col) & (owner_row != last))
         index_v[tile] = jnp.where(lists < 0, 0, jnp.where(full, 1 + lists, ranked))
     index_copy = pltpu.make_async_copy(index_v, index_s, load_sem.at[INDEX])
     index_copy.start()
@@ -303,16 +324,19 @@
     away = (block - (me * nb + iota((nb, keys), 0))) * BLK + lane % BLK
     kp_s[...] = jnp.where(block < 0, 1 << 24, away).astype(F32)
 
-    choose_a(z, lambda z, y, hop: y == 0, lambda z, y, hop: y < N_Y - 1, lambda z, y, hop: y < N_Y - 2)
-    choose_b(z, lambda z, y, hop: (y == 1) | (y == 2))
-
-    routes = (((0, 1), y, reach_a, back_a), ((2,), left_col, reach_b, back_b))
+    choose_1(z, lambda z, y, hop: y == 0, lambda z, y, hop: y < N_Y - 1, lambda z, y, hop: y < N_Y - 2)
+    choose_0(z, lambda z, y, hop: y == 0)
+    choose_last(
+        lambda z, y, hop: (z == last) & (y < N_Y - 1), lambda z, y, hop: (z == last) & (y < N_Y - 2))
+    choose_2(z, lambda z, y, hop: (z < last) & ((y == 1) | (y == 2)))
+
+    routes = ((1, y, reach_a, back_a), (0, y, reach_a, back_a), (2, left_col, reach_b, back_b))
     hops = range(1, n_z // 2 + 1)
 
     def one_hop(hop, carry):
         above = lax.max(z - hop, 0)
         below = lax.rem(z + hop, n_z)
-        for kinds, col, reach, back in routes:
+        for kind, col, reach, back in routes:
 
             def from_above(z, y, hop, reach=reach):
                 return (z >= hop) & (hop <= reach)
@@ -329,16 +353,17 @@
             def use_below(z, y, hop, back=back):
                 return ((z + hop) % n_z < back) & (hop <= back) & ((z + hop) % n_z < z)
 
-            for kind in kinds:
-                arrive(kind, above, col, from_above, hop)
-                send_whole(UP, kind, above, col, go_up, hop)
-                arrive(kind, below, col, from_below, hop)
-                send_whole(DOWN, kind, below, col, go_down, hop)
+            arrive(kind, above, col, from_above, hop)
+            send_whole(UP, kind, above, col, go_up, hop)
+            arrive(kind, below, col, from_below, hop)
+            send_whole(DOWN, kind, below, col, go_down, hop)
             for row, use in ((above, from_above), (below, use_below)):
-                if len(kinds) == 2:
-                    choose_a(row, use, use, use, hop)
+                if kind == 1:
+                    choose_1(row, use, use, use, hop)
+                elif kind == 0:
+                    choose_0(row, use, hop)
                 else:
-                    choose_b(row, use, hop)
+                    choose_2(row, use, hop)
         return carry
 
     lax.fori_loop(hops.start, hops.stop, one_hop, 0)
@@ -352,11 +377,17 @@
                     if units:
                         @pl.when(y == j)
                         def _():
-                            part = kv.at[:, 0:units * MOST // 2]
+                            part = kv0.at[0:units * MOST]
                             pltpu.make_async_copy(part, part, sem).wait()
 
-    settle(lambda z, y: 2 * (z + (y == N_Y - 1)) + (z + (y >= 1)) + 2 * (z + (y >= 2)), end_sem.at[0])
-    index_copy.wait()
+    def due(tile):
+        def count(z, y):
+            if tile == 1:
+                return (z + (y == N_Y - 1)) + (z + (y >= 1)) + (z + (y >= 2))
+            if z == last:
+                return (z + (y == N_Y - 1)) + z + (y >= 1) + (y >= 2)
+            return (z + (y == N_Y - 1)) + (z + (y >= 2))
+        return count
 
     query_row = iota((BLK, keys), 0).astype(F32)
     ones = jnp.ones((keys, LANES), BF16)
@@ -367,20 +398,19 @@
     def slope_of(head):
         return core_slope * (2.0 ** (-8.0 * (head + 1) / n_heads))
 
-    def attend(r):
+    def attend(r, side):
         key_pos = kp_s[pl.ds(r, 1), :]
         allowed = key_pos <= query_row
-        outs = []
-        for side in range(kv_heads):
-            both = jnp.concatenate([kv[side, index_s[side, r, e]] for e in range(entries)], axis=0)
-            scores = dot_nt(q_s[r, side * group * BLK:(side + 1) * group * BLK], both)
-            weights = []
-            for t in range(group):
-                bias = key_pos * (slope_of(side * group + t) * (alibi * LOG2E))
-                part = jnp.exp2(scores[t * BLK:(t + 1) * BLK] + bias)
-                weights.append(jnp.where(allowed, part, 0.0).astype(BF16))
-            outs.append(dot(jnp.concatenate(weights, axis=0), jnp.concatenate([both, ones], axis=1)))
-
+        both = jnp.concatenate([kv[side][index_s[side, r, e]] for e in range(entries)], axis=0)
+        scores = dot_nt(q_s[r, side * group * BLK:(side + 1) * group * BLK], both)
+        weights = []
+        for t in range(group):
+            bias = key_pos * (slope_of(side * group + t) * (alibi * LOG2E))
+            part = jnp.exp2(scores[t * BLK:(t + 1) * BLK] + bias)
+            weights.append(jnp.where(allowed, part, 0.0).astype(BF16))
+        return dot(jnp.concatenate(weights, axis=0), jnp.concatenate([both, ones], axis=1))
+
+    def combine(r, outs):
         sums = jnp.ones((BLK, LANES), F32)
         at = pl.ds(pl.multiple_of(r * BLK, BLK), BLK)
         for t in range(group):
@@ -405,13 +435,24 @@
             device_id={"tp": partner}, device_id_type=MESH)
 
     def one_part(part, carry):
-        for r in range(nb // PARTS):
-            attend(part * (nb // PARTS) + r)
+        for i in range(nb // PARTS):
+            r = part * (nb // PARTS) + i
+            combine(r, (attend(r, 0), found_s[r]))
         at = part_at(part)
         part_send[at] = dot(att_s[at], wo_buf[1]).astype(BF16)
         part_copy(part).start()
         return carry
 
+    def second_head(part, carry):
+        for i in range(nb // PARTS):
+            r = part * (nb // PARTS) + i
+            found_s[r] = attend(r, 1)
+        return carry
+
+    index_copy.wait()
+    settle(due(1), end_sem.at[1])
+    lax.fori_loop(0, PARTS, second_head, 0)
+    settle(due(0), end_sem.at[0])
     lax.fori_loop(0, PARTS, one_part, 0)
 
     own = dot(att_s[...], wo_buf[0])
@@ -420,12 +461,13 @@
     logs = jnp.log(sum_s[...]) - slopes * alibi * row_in
     lt_ref[...] = logs.T[0:heads]
 
-    def all_sent(z, y):
-        return sum(
-            units for units, when, looped in sent
+    def all_sent(size):
+        return lambda z, y: sum(
+            units for units, when, looped in sent if units == size
             for hop in (hops if looped else (0,)) if when(z, y, hop))
 
-    settle(all_sent, send_sem.at[0])
+    for chain in range(2):
+        settle(all_sent(2 - chain), send_sem.at[chain])
 
     for part in range(PARTS):
         at = slice(part * part_rows, (part + 1) * part_rows)
@@ -472,10 +514,12 @@
             pltpu.SMEM((2, nb, entries), jnp.int32),
             vmem((n_z, 2, MOST, BLK, LANES), BF16),
             vmem((n_z, 2, MOST, BLK, LANES), BF16),
-            vmem((n_z, MOST, BLK, LANES), BF16),
+            vmem((n_z, 2, MOST, BLK, LANES), BF16),
             vmem((nb, heads * BLK, LANES), BF16),
-            vmem((2, 1 + n_kv * nb, BLK, LANES), BF16),
+            vmem((1 + n_kv * nb, BLK, LANES), BF16),
+            vmem((1 + n_kv * nb, BLK, LANES), BF16),
             vmem((nb, entries * BLK), F32),
+            vmem((nb, heads // 2 * BLK, 2 * LANES), F32),
             vmem((rows, q_cols), BF16),
             vmem((rows, LANES), F32),
             vmem((rows, half), BF16),
@@ -483,9 +527,9 @@
             dma((8,)),
             dma((2,)),
             dma((2, 3)),
-            dma((1,)),
+            dma((2,)),
             dma((3, n_z)),
-            dma((1,)),
+            dma((2,)),
             dma((2, PARTS)),
         ],
         compiler_params=pltpu.CompilerParams(

time: 33.5 us -> 32.9 us (0.982)
  Pallas kernels: 32.8 us -> 32.2 us
    pallas_call x1, Pallas kernels: 32.1 us -> 31.5 us  [shards(): pl.pallas_call(functools.partial(kernel, n_kv), out_shape=(vmem((rows, ha...]
where the time goes in v4:
time: 32.9 us; the launch traced here: 32.8 us
  Pallas kernels  32.2 us (98%)
  between operations  0.64 us (2%)
    pallas_call x1, Pallas kernels, shards(): pl.pallas_call(functools.partial(kernel, n_kv), out_shape=(vmem((rows, ha...  31.5 us
    pallas_call x1, Pallas kernels, shards(): pl.pallas_call(write_out, out_shape=(jax.ShapeDtypeStruct((rows, half), B...  0.72 us

profile of v4, /device:TPU:193, one launch (start us, length us, event | category | flops | bytes accessed | tf_op | source)
XLA Modules:
  0.0 32.8 jit_solution(13330859477107628536)
XLA Ops:
  0.6 31.5 %shard_map.104 = (bf16[256,512]{1,0:T(8,128)(2,1)S(1)}, f32[8,256]{1,0:T(8,128)S(1)}) custom-call(bf16[256,512]{1,0:T(8,128)(2,1)} %bitcast.7, f32[1,1024]{1,0:T(1,128)} %bitcast.8, bf16[1024,512]{1,0:T(8,128)(2,1)} %wq.1, bf16[1024,128]{1,0:T(8,128)(2,1)} %wk.1, bf16[1024,128]{1,0:T(8,128)(2,1)} %wv.1, f32[1,64]{1,0:T(1,128)} %bitcast.10, ...), custom_call_target="tpu_custom_call" | custom-call | tf_op jit(solution)/shard_map/pallas_call | solution.py:497
  32.1 0.7 %shard_map.105 = (bf16[256,512]{1,0:T(8,128)(2,1)}, f32[8,256]{1,0:T(8,128)}) custom-call(bf16[256,512]{1,0:T(8,128)(2,1)S(1)} %get-tuple-element.6.mixed, f32[8,256]{1,0:T(8,128)S(1)} %get-tuple-element.7.log_total), custom_call_target="tpu_custom_call" | custom-call | tf_op jit(solution)/shard_map/pallas_call | solution.py:542

commit v5 on v4

--- a/solution.py
+++ b/solution.py
@@ -286,10 +286,6 @@
             for r in range(nb):
                 q_s[r, head * BLK:(head + 1) * BLK] = here[r * BLK:(r + 1) * BLK]
 
-    arrive(2, z, left_col, lambda z, y, hop: z < last)
-    send_whole(UP, 2, z, left_col, lambda z, y, hop: z < last)
-    send_whole(DOWN, 2, z, left_col, lambda z, y, hop: z < back_b)
-
     for copy in place_copies:
         copy.wait()
     spread = jnp.where(
@@ -324,6 +320,9 @@
     away = (block - (me * nb + iota((nb, keys), 0))) * BLK + lane % BLK
     kp_s[...] = jnp.where(block < 0, 1 << 24, away).astype(F32)
 
+    arrive(2, z, left_col, lambda z, y, hop: z < last)
+    send_whole(UP, 2, z, left_col, lambda z, y, hop: z < last)
+    send_whole(DOWN, 2, z, left_col, lambda z, y, hop: z < back_b)
     choose_1(z, lambda z, y, hop: y == 0, lambda z, y, hop: y < N_Y - 1, lambda z, y, hop: y < N_Y - 2)
     choose_0(z, lambda z, y, hop: y == 0)
     choose_last(

time: 32.9 us -> 32.9 us (level)
  no operation moved by 1% of the time
where the time goes in v5:
time: 32.9 us; the launch traced here: 32.8 us
  Pallas kernels  32.2 us (98%)
  between operations  0.64 us (2%)
    pallas_call x1, Pallas kernels, shards(): pl.pallas_call(functools.partial(kernel, n_kv), out_shape=(vmem((rows, ha...  31.5 us
    pallas_call x1, Pallas kernels, shards(): pl.pallas_call(write_out, out_shape=(jax.ShapeDtypeStruct((rows, half), B...  0.72 us

profile of v5, /device:TPU:193, one launch (start us, length us, event | category | flops | bytes accessed | tf_op | source)
XLA Modules:
  0.0 32.8 jit_solution(12805989531543234273)
XLA Ops:
  0.6 31.5 %shard_map.104 = (bf16[256,512]{1,0:T(8,128)(2,1)S(1)}, f32[8,256]{1,0:T(8,128)S(1)}) custom-call(bf16[256,512]{1,0:T(8,128)(2,1)} %bitcast.7, f32[1,1024]{1,0:T(1,128)} %bitcast.8, bf16[1024,512]{1,0:T(8,128)(2,1)} %wq.1, bf16[1024,128]{1,0:T(8,128)(2,1)} %wk.1, bf16[1024,128]{1,0:T(8,128)(2,1)} %wv.1, f32[1,64]{1,0:T(1,128)} %bitcast.10, ...), custom_call_target="tpu_custom_call" | custom-call | tf_op jit(solution)/shard_map/pallas_call | solution.py:496
  32.1 0.7 %shard_map.105 = (bf16[256,512]{1,0:T(8,128)(2,1)}, f32[8,256]{1,0:T(8,128)}) custom-call(bf16[256,512]{1,0:T(8,128)(2,1)S(1)} %get-tuple-element.6.mixed, f32[8,256]{1,0:T(8,128)S(1)} %get-tuple-element.7.log_total), custom_call_target="tpu_custom_call" | custom-call | tf_op jit(solution)/shard_map/pallas_call | solution.py:541

commit v6 on v5

--- a/solution.py
+++ b/solution.py
@@ -183,9 +183,8 @@
     back_a, back_b = last - reach_a, last - reach_b
     sent = []
 
-    def send(direction, src, dst, units, arrival, when, hop=None):
-        chain = 0 if units == 2 else 1
-        sent.append((units, when, hop is not None))
+    def send(direction, src, dst, chain, units, arrival, when, hop=None):
+        sent.append((chain, units, when, hop is not None))
 
         @pl.when(when(z, y, hop))
         def _():
@@ -196,15 +195,14 @@
     def stage(kind, row):
         return stage_sem.at[kind, row]
 
-    def tile_of(kind):
-        return kind % 2
-
     def whole(kind, row, col):
-        return kv[tile_of(kind)].at[pl.ds(base(row, col), nb)]
+        if kind < 2:
+            return kv[kind].at[pl.ds(base(row, col), nb)]
+        return kv0.at[pl.ds(base(row, col) + (kind - 2) * (nb // 2), nb // 2)]
 
     def send_whole(direction, kind, row, col, when, hop=None):
         part = whole(kind, row, col)
-        send(direction, part, part, 2, stage(kind, row), when, hop)
+        send(direction, part, part, 0, 2 if kind < 2 else 1, stage(kind, row), when, hop)
 
     def arrive(kind, row, col, when, hop=None):
         @pl.when(when(z, y, hop))
@@ -221,14 +219,14 @@
         code = code_s[which, pl.ds(row, 1), :]
         return jnp.where(same_row & (code == row_slot), 1.0, 0.0).astype(BF16)
 
-    def item(kind, row, col):
-        return kv[tile_of(kind)][pl.ds(base(row, col), nb)].reshape(rows, LANES)
+    def item(tile, row, col):
+        return kv[tile][pl.ds(base(row, col), nb)].reshape(rows, LANES)
 
     def blocks(x):
         return x.astype(BF16).reshape(-1, BLK, LANES)
 
     def send_chosen(direction, buf, tile, row, col, when, hop=None):
-        send(direction, buf, kv[tile].at[pl.ds(base(row, col), MOST)], 1, end_sem.at[tile], when, hop)
+        send(direction, buf, kv[tile].at[pl.ds(base(row, col), MOST)], 1, 1, end_sem.at[tile], when, hop)
 
     def choose_1(row, to_left, to_right, to_far, hop=None):
         @pl.when(to_left(z, y, hop) | to_right(z, y, hop) | to_far(z, y, hop))
@@ -253,7 +251,7 @@
     def choose_2(row, to_right, hop=None):
         @pl.when(to_right(z, y, hop))
         def _():
-            right_s[row, 0] = blocks(dot(chooser(3, row), item(2, row, left_col)))
+            right_s[row, 0] = blocks(dot(chooser(3, row), item(0, row, left_col)))
 
         send_chosen(RIGHT, right_s.at[row, 0], 0, row, left_col, to_right, hop)
 
@@ -269,7 +267,8 @@
         send_chosen(RIGHT, right_s.at[z, 0], 0, z, y, to_right)
 
     left_col = lax.rem(y + N_Y - 1, N_Y)
-    send(RIGHT, whole(0, z, y), whole(0, z, y), 2, stage(2, z), lambda z, y, hop: z < last)
+    for kind in (2, 3):
+        send_whole(RIGHT, kind, z, y, lambda z, y, hop: z < last)
     for kind in (1, 0):
         send_whole(UP, kind, z, y, lambda z, y, hop: z < last)
         send_whole(DOWN, kind, z, y, lambda z, y, hop: z < back_a)
@@ -320,22 +319,23 @@
     away = (block - (me * nb + iota((nb, keys), 0))) * BLK + lane % BLK
     kp_s[...] = jnp.where(block < 0, 1 << 24, away).astype(F32)
 
-    arrive(2, z, left_col, lambda z, y, hop: z < last)
-    send_whole(UP, 2, z, left_col, lambda z, y, hop: z < last)
-    send_whole(DOWN, 2, z, left_col, lambda z, y, hop: z < back_b)
+    for kind in (2, 3):
+        arrive(kind, z, left_col, lambda z, y, hop: z < last)
+        send_whole(UP, kind, z, left_col, lambda z, y, hop: z < last)
+        send_whole(DOWN, kind, z, left_col, lambda z, y, hop: z < back_b)
     choose_1(z, lambda z, y, hop: y == 0, lambda z, y, hop: y < N_Y - 1, lambda z, y, hop: y < N_Y - 2)
     choose_0(z, lambda z, y, hop: y == 0)
     choose_last(
         lambda z, y, hop: (z == last) & (y < N_Y - 1), lambda z, y, hop: (z == last) & (y < N_Y - 2))
     choose_2(z, lambda z, y, hop: (z < last) & ((y == 1) | (y == 2)))
 
-    routes = ((1, y, reach_a, back_a), (0, y, reach_a, back_a), (2, left_col, reach_b, back_b))
+    routes = (((1,), y, reach_a, back_a), ((0,), y, reach_a, back_a), ((2, 3), left_col, reach_b, back_b))
     hops = range(1, n_z // 2 + 1)
 
     def one_hop(hop, carry):
         above = lax.max(z - hop, 0)
         below = lax.rem(z + hop, n_z)
-        for kind, col, reach, back in routes:
+        for kinds, col, reach, back in routes:
 
             def from_above(z, y, hop, reach=reach):
                 return (z >= hop) & (hop <= reach)
@@ -352,14 +352,15 @@
             def use_below(z, y, hop, back=back):
                 return ((z + hop) % n_z < back) & (hop <= back) & ((z + hop) % n_z < z)
 
-            arrive(kind, above, col, from_above, hop)
-            send_whole(UP, kind, above, col, go_up, hop)
-            arrive(kind, below, col, from_below, hop)
-            send_whole(DOWN, kind, below, col, go_down, hop)
+            for kind in kinds:
+                arrive(kind, above, col, from_above, hop)
+                send_whole(UP, kind, above, col, go_up, hop)
+                arrive(kind, below, col, from_below, hop)
+                send_whole(DOWN, kind, below, col, go_down, hop)
             for row, use in ((above, from_above), (below, use_below)):
-                if kind == 1:
+                if kinds == (1,):
                     choose_1(row, use, use, use, hop)
-                elif kind == 0:
+                elif kinds == (0,):
                     choose_0(row, use, hop)
                 else:
                     choose_2(row, use, hop)
@@ -460,13 +461,13 @@
     logs = jnp.log(sum_s[...]) - slopes * alibi * row_in
     lt_ref[...] = logs.T[0:heads]
 
-    def all_sent(size):
+    def all_sent(which):
         return lambda z, y: sum(
-            units for units, when, looped in sent if units == size
+            units for chain, units, when, looped in sent if chain == which
             for hop in (hops if looped else (0,)) if when(z, y, hop))
 
     for chain in range(2):
-        settle(all_sent(2 - chain), send_sem.at[chain])
+        settle(all_sent(chain), send_sem.at[chain])
 
     for part in range(PARTS):
         at = slice(part * part_rows, (part + 1) * part_rows)
@@ -527,7 +528,7 @@
             dma((2,)),
             dma((2, 3)),
             dma((2,)),
-            dma((3, n_z)),
+            dma((4, n_z)),
             dma((2,)),
             dma((2, PARTS)),
         ],

time: 32.9 us -> 32.9 us (level); the launches traced: 32.8 us -> 32.3 us
  Pallas kernels: 32.2 us -> 31.7 us
    pallas_call x1, Pallas kernels: 31.5 us -> 31 us  [shards(): pl.pallas_call(functools.partial(kernel, n_kv), out_shape=(vmem((rows, ha...]
where the time goes in v6:
time: 32.9 us; the launch traced here: 32.3 us
  Pallas kernels  31.7 us (96%)
  between operations  0.64 us (2%)
    pallas_call x1, Pallas kernels, shards(): pl.pallas_call(functools.partial(kernel, n_kv), out_shape=(vmem((rows, ha...  31 us
    pallas_call x1, Pallas kernels, shards(): pl.pallas_call(write_out, out_shape=(jax.ShapeDtypeStruct((rows, half), B...  0.72 us

profile of v6, /device:TPU:193, one launch (start us, length us, event | category | flops | bytes accessed | tf_op | source)
XLA Modules:
  0.0 32.3 jit_solution(6973153942744895355)
XLA Ops:
  0.6 31.0 %shard_map.104 = (bf16[256,512]{1,0:T(8,128)(2,1)S(1)}, f32[8,256]{1,0:T(8,128)S(1)}) custom-call(bf16[256,512]{1,0:T(8,128)(2,1)} %bitcast.7, f32[1,1024]{1,0:T(1,128)} %bitcast.8, bf16[1024,512]{1,0:T(8,128)(2,1)} %wq.1, bf16[1024,128]{1,0:T(8,128)(2,1)} %wk.1, bf16[1024,128]{1,0:T(8,128)(2,1)} %wv.1, f32[1,64]{1,0:T(1,128)} %bitcast.10, ...), custom_call_target="tpu_custom_call" | custom-call | tf_op jit(solution)/shard_map/pallas_call | solution.py:497
  31.6 0.7 %shard_map.105 = (bf16[256,512]{1,0:T(8,128)(2,1)}, f32[8,256]{1,0:T(8,128)}) custom-call(bf16[256,512]{1,0:T(8,128)(2,1)S(1)} %get-tuple-element.6.mixed, f32[8,256]{1,0:T(8,128)S(1)} %get-tuple-element.7.log_total), custom_call_target="tpu_custom_call" | custom-call | tf_op jit(solution)/shard_map/pallas_call | solution.py:542

commit v7 on v5

--- a/solution.py
+++ b/solution.py
@@ -411,7 +411,7 @@
 
     def combine(r, outs):
         sums = jnp.ones((BLK, LANES), F32)
-        at = pl.ds(pl.multiple_of(r * BLK, BLK), BLK)
+        at = pl.ds(r * BLK, BLK)
         for t in range(group):
             first, second = (o[t * BLK:(t + 1) * BLK] for o in outs)
             top = jnp.where(tile_low, first[:, 0:LANES], second[:, 0:LANES])
@@ -425,7 +425,7 @@
     part_rows = rows // PARTS
 
     def part_at(part):
-        return pl.ds(pl.multiple_of(part * part_rows, part_rows), part_rows)
+        return pl.ds(part * part_rows, part_rows)
 
     def part_copy(part):
         at = part_at(part)
@@ -433,26 +433,21 @@
             part_send.at[at], part_recv.at[at], part_sem.at[0, part], part_sem.at[1, part],
             device_id={"tp": partner}, device_id_type=MESH)
 
-    def one_part(part, carry):
+    def one_part(part):
         for i in range(nb // PARTS):
             r = part * (nb // PARTS) + i
             combine(r, (attend(r, 0), found_s[r]))
         at = part_at(part)
         part_send[at] = dot(att_s[at], wo_buf[1]).astype(BF16)
         part_copy(part).start()
-        return carry
-
-    def second_head(part, carry):
-        for i in range(nb // PARTS):
-            r = part * (nb // PARTS) + i
-            found_s[r] = attend(r, 1)
-        return carry
 
     index_copy.wait()
     settle(due(1), end_sem.at[1])
-    lax.fori_loop(0, PARTS, second_head, 0)
+    for r in range(nb):
+        found_s[r] = attend(r, 1)
     settle(due(0), end_sem.at[0])
-    lax.fori_loop(0, PARTS, one_part, 0)
+    for part in range(PARTS):
+        one_part(part)
 
     own = dot(att_s[...], wo_buf[0])
     row_in = (iota((rows, LANES), 0) % BLK).astype(F32)

time: 32.9 us -> 32.9 us (level)
  no operation moved by 1% of the time
where the time goes in v7:
time: 32.9 us; the launch traced here: 32.8 us
  Pallas kernels  32.1 us (98%)
  between operations  0.64 us (2%)
    pallas_call x1, Pallas kernels, shards(): pl.pallas_call(functools.partial(kernel, n_kv), out_shape=(vmem((rows, ha...  31.4 us
    pallas_call x1, Pallas kernels, shards(): pl.pallas_call(write_out, out_shape=(jax.ShapeDtypeStruct((rows, half), B...  0.72 us

profile of v7, /device:TPU:193, one launch (start us, length us, event | category | flops | bytes accessed | tf_op | source)
XLA Modules:
  0.0 32.8 jit_solution(3372766127165146801)
XLA Ops:
  0.6 31.4 %shard_map.104 = (bf16[256,512]{1,0:T(8,128)(2,1)S(1)}, f32[8,256]{1,0:T(8,128)S(1)}) custom-call(bf16[256,512]{1,0:T(8,128)(2,1)} %bitcast.7, f32[1,1024]{1,0:T(1,128)} %bitcast.8, bf16[1024,512]{1,0:T(8,128)(2,1)} %wq.1, bf16[1024,128]{1,0:T(8,128)(2,1)} %wk.1, bf16[1024,128]{1,0:T(8,128)(2,1)} %wv.1, f32[1,64]{1,0:T(1,128)} %bitcast.10, ...), custom_call_target="tpu_custom_call" | custom-call | tf_op jit(solution)/shard_map/pallas_call | solution.py:491
  32.0 0.7 %shard_map.105 = (bf16[256,512]{1,0:T(8,128)(2,1)}, f32[8,256]{1,0:T(8,128)}) custom-call(bf16[256,512]{1,0:T(8,128)(2,1)S(1)} %get-tuple-element.6.mixed, f32[8,256]{1,0:T(8,128)S(1)} %get-tuple-element.7.log_total), custom_call_target="tpu_custom_call" | custom-call | tf_op jit(solution)/shard_map/pallas_call | solution.py:536

commit v8 on v6

--- a/solution.py
+++ b/solution.py
@@ -273,6 +273,21 @@
         send_whole(UP, kind, z, y, lambda z, y, hop: z < last)
         send_whole(DOWN, kind, z, y, lambda z, y, hop: z < back_a)
 
+    for copy in place_copies:
+        copy.wait()
+    spread = jnp.where(
+        iota((n_blocks, rows), 0) % nb == iota((n_blocks, rows), 1) // BLK, 1.0, 0.0).astype(BF16)
+    row_owner = iota((n_z, n_blocks), 0) * N_Y
+    owner_lane = iota((n_z, n_blocks), 1) // nb
+    for which, (slot, col) in enumerate(((0, y), (1, y), (2, y), (1, left_col))):
+        mine = jnp.where(owner_lane == row_owner + col, place_recv[slot], 0.0)
+        code_s[which] = dot(mine.astype(BF16), spread)
+
+    choose_1(z, lambda z, y, hop: y == 0, lambda z, y, hop: y < N_Y - 1, lambda z, y, hop: y < N_Y - 2)
+    choose_0(z, lambda z, y, hop: y == 0)
+    choose_last(
+        lambda z, y, hop: (z == last) & (y < N_Y - 1), lambda z, y, hop: (z == last) & (y < N_Y - 2))
+
     raw = (raw_s[:, 0:q_cols] + dot(y1, w_buf[1, :, 0:q_cols])) * row_scale
     for tile in range(q_cols // LANES):
         q = head_norm(raw[:, tile * LANES:(tile + 1) * LANES], qg_row)
@@ -284,16 +299,6 @@
             here = jnp.where(low if side == 1 else ~low, here, 0.0).astype(BF16)
             for r in range(nb):
                 q_s[r, head * BLK:(head + 1) * BLK] = here[r * BLK:(r + 1) * BLK]
-
-    for copy in place_copies:
-        copy.wait()
-    spread = jnp.where(
-        iota((n_blocks, rows), 0) % nb == iota((n_blocks, rows), 1) // BLK, 1.0, 0.0).astype(BF16)
-    row_owner = iota((n_z, n_blocks), 0) * N_Y
-    owner_lane = iota((n_z, n_blocks), 1) // nb
-    for which, (slot, col) in enumerate(((0, y), (1, y), (2, y), (1, left_col))):
-        mine = jnp.where(owner_lane == row_owner + col, place_recv[slot], 0.0)
-        code_s[which] = dot(mine.astype(BF16), spread)
 
     lane_entry = iota((nb, entries), 1)
     rank = jnp.zeros((nb, entries), jnp.int32)
@@ -323,10 +328,6 @@
         arrive(kind, z, left_col, lambda z, y, hop: z < last)
         send_whole(UP, kind, z, left_col, lambda z, y, hop: z < last)
         send_whole(DOWN, kind, z, left_col, lambda z, y, hop: z < back_b)
-    choose_1(z, lambda z, y, hop: y == 0, lambda z, y, hop: y < N_Y - 1, lambda z, y, hop: y < N_Y - 2)
-    choose_0(z, lambda z, y, hop: y == 0)
-    choose_last(
-        lambda z, y, hop: (z == last) & (y < N_Y - 1), lambda z, y, hop: (z == last) & (y < N_Y - 2))
     choose_2(z, lambda z, y, hop: (z < last) & ((y == 1) | (y == 2)))
 
     routes = (((1,), y, reach_a, back_a), ((0,), y, reach_a, back_a), ((2, 3), left_col, reach_b, back_b))
@@ -412,7 +413,7 @@
 
     def combine(r, outs):
         sums = jnp.ones((BLK, LANES), F32)
-        at = pl.ds(pl.multiple_of(r * BLK, BLK), BLK)
+        at = pl.ds(r * BLK, BLK)
         for t in range(group):
             first, second = (o[t * BLK:(t + 1) * BLK] for o in outs)
             top = jnp.where(tile_low, first[:, 0:LANES], second[:, 0:LANES])
@@ -426,7 +427,7 @@
     part_rows = rows // PARTS
 
     def part_at(part):
-        return pl.ds(pl.multiple_of(part * part_rows, part_rows), part_rows)
+        return pl.ds(part * part_rows, part_rows)
 
     def part_copy(part):
         at = part_at(part)
@@ -434,26 +435,24 @@
             part_send.at[at], part_recv.at[at], part_sem.at[0, part], part_sem.at[1, part],
             device_id={"tp": partner}, device_id_type=MESH)
 
-    def one_part(part, carry):
-        for i in range(nb // PARTS):
-            r = part * (nb // PARTS) + i
-            combine(r, (attend(r, 0), found_s[r]))
+    def one_part(part):
+        each = nb // PARTS
+        first = [attend(part * each + i, 0) for i in range(each)]
+        for i in range(each):
+            combine(part * each + i, (first[i], found_s[part * each + i]))
         at = part_at(part)
         part_send[at] = dot(att_s[at], wo_buf[1]).astype(BF16)
         part_copy(part).start()
-        return carry
-
-    def second_head(part, carry):
-        for i in range(nb // PARTS):
-            r = part * (nb // PARTS) + i
-            found_s[r] = attend(r, 1)
-        return carry
 
     index_copy.wait()
     settle(due(1), end_sem.at[1])
-    lax.fori_loop(0, PARTS, second_head, 0)
+    for start in range(0, nb, 4):
+        second = [attend(start + i, 1) for i in range(4)]
+        for i in range(4):
+            found_s[start + i] = second[i]
     settle(due(0), end_sem.at[0])
-    lax.fori_loop(0, PARTS, one_part, 0)
+    for part in range(PARTS):
+        one_part(part)
 
     own = dot(att_s[...], wo_buf[0])
     row_in = (iota((rows, LANES), 0) % BLK).astype(F32)

time: 32.9 us -> 32.5 us (0.988)
  no operation moved by 1% of the time
where the time goes in v8:
time: 32.5 us; the launch traced here: 32.3 us
  Pallas kernels  31.6 us (97%)
  between operations  0.64 us (2%)
    pallas_call x1, Pallas kernels, shards(): pl.pallas_call(functools.partial(kernel, n_kv), out_shape=(vmem((rows, ha...  30.9 us
    pallas_call x1, Pallas kernels, shards(): pl.pallas_call(write_out, out_shape=(jax.ShapeDtypeStruct((rows, half), B...  0.72 us

profile of v8, /device:TPU:193, one launch (start us, length us, event | category | flops | bytes accessed | tf_op | source)
XLA Modules:
  0.0 32.3 jit_solution(10421356020538275222)
XLA Ops:
  0.6 30.9 %shard_map.104 = (bf16[256,512]{1,0:T(8,128)(2,1)S(1)}, f32[8,256]{1,0:T(8,128)S(1)}) custom-call(bf16[256,512]{1,0:T(8,128)(2,1)} %bitcast.7, f32[1,1024]{1,0:T(1,128)} %bitcast.8, bf16[1024,512]{1,0:T(8,128)(2,1)} %wq.1, bf16[1024,128]{1,0:T(8,128)(2,1)} %wk.1, bf16[1024,128]{1,0:T(8,128)(2,1)} %wv.1, f32[1,64]{1,0:T(1,128)} %bitcast.10, ...), custom_call_target="tpu_custom_call" | custom-call | tf_op jit(solution)/shard_map/pallas_call | solution.py:496
  31.5 0.7 %shard_map.105 = (bf16[256,512]{1,0:T(8,128)(2,1)}, f32[8,256]{1,0:T(8,128)}) custom-call(bf16[256,512]{1,0:T(8,128)(2,1)S(1)} %get-tuple-element.6.mixed, f32[8,256]{1,0:T(8,128)S(1)} %get-tuple-element.7.log_total), custom_call_target="tpu_custom_call" | custom-call | tf_op jit(solution)/shard_map/pallas_call | solution.py:541

commit v9 on v8

--- a/solution.py
+++ b/solution.py
@@ -12,6 +12,7 @@
 BLK = 32
 LANES = 128
 MOST = 4
+LATE = 4
 PARTS = 2
 N_Y = 4
 UP, DOWN, LEFT, RIGHT, FAR = range(5)
@@ -43,7 +44,7 @@
     out_ref, lt_ref,
     x_buf, ch_buf, raw_s, w_buf, wo_buf, g_buf, hg_buf,
     place_send, place_recv, code_s, index_v, index_s, left_s, right_s, far_s,
-    q_s, kv0, kv1, kp_s, found_s, att_s, sum_s, part_send, part_recv,
+    q_s, kv0, kv1, late_s, kp_s, late_kp, found_s, att_s, sum_s, part_send, part_recv,
     load_sem, x_sem, place_sem, send_sem, stage_sem, end_sem, part_sem,
 ):
     me = lax.axis_index("kv")
@@ -181,6 +182,12 @@
     last = n_z - 1
     reach_a, reach_b = n_z // 2, n_z // 2 - 1
     back_a, back_b = last - reach_a, last - reach_b
+    assert LATE == reach_a == back_b
+
+    @pl.when(z < LATE)
+    def _():
+        late_s[...] = jnp.zeros(late_s.shape, BF16)
+
     sent = []
 
     def send(direction, src, dst, chain, units, arrival, when, hop=None):
@@ -241,19 +248,27 @@
         send_chosen(LEFT, left_s.at[row, 1], 1, row, y, to_left, hop)
         send_chosen(RIGHT, right_s.at[row, 1], 1, row, y, to_right, hop)
 
+    def send_tile_0(direction, buf, slot, row, col, when, hop):
+        if hop is None:
+            send_chosen(direction, buf, 0, row, col, when)
+            return
+        send_chosen(direction, buf, 0, row, col, lambda z, y, hop: when(z, y, hop) & (hop < LATE), hop)
+        send(direction, buf, late_s.at[slot], 1, 1, end_sem.at[2],
+             lambda z, y, hop: when(z, y, hop) & (hop == LATE), hop)
+
     def choose_0(row, to_left, hop=None):
         @pl.when(to_left(z, y, hop))
         def _():
             left_s[row, 0] = blocks(dot(chooser(0, row), item(0, row, y)))
 
-        send_chosen(LEFT, left_s.at[row, 0], 0, row, y, to_left, hop)
+        send_tile_0(LEFT, left_s.at[row, 0], 0, row, y, to_left, hop)
 
     def choose_2(row, to_right, hop=None):
         @pl.when(to_right(z, y, hop))
         def _():
             right_s[row, 0] = blocks(dot(chooser(3, row), item(0, row, left_col)))
 
-        send_chosen(RIGHT, right_s.at[row, 0], 0, row, left_col, to_right, hop)
+        send_tile_0(RIGHT, right_s.at[row, 0], 1, row, left_col, to_right, hop)
 
     def choose_last(to_right, to_far):
         @pl.when(to_right(z, y, None))
@@ -309,11 +324,16 @@
     owner_row = owner // N_Y
     col = lax.rem(owner, N_Y)
     ranked = 1 + owner * nb + rank
+    late_owners = [
+        jnp.where(z >= LATE, (z - LATE) * N_Y + lax.rem(y + step, N_Y), -2) for step in (1, 2)]
     for tile in range(2):
         full = col == y
         if tile == 0:
             full = full | ((col == left_col) & (owner_row != last))
-        index_v[tile] = jnp.where(lists < 0, 0, jnp.where(full, 1 + lists, ranked))
+        empty = lists < 0
+        if tile == 0:
+            empty = empty | (owner == late_owners[0]) | (owner == late_owners[1])
+        index_v[tile] = jnp.where(empty, 0, jnp.where(full, 1 + lists, ranked))
     index_copy = pltpu.make_async_copy(index_v, index_s, load_sem.at[INDEX])
     index_copy.start()
 
@@ -321,8 +341,22 @@
     block = jnp.full((nb, keys), -1, jnp.int32)
     for e in range(entries):
         block = jnp.where(lane // BLK == e, lists[:, e:e + 1], block)
-    away = (block - (me * nb + iota((nb, keys), 0))) * BLK + lane % BLK
-    kp_s[...] = jnp.where(block < 0, 1 << 24, away).astype(F32)
+    block_owner = block // nb
+    late = (block_owner == late_owners[0]) | (block_owner == late_owners[1])
+
+    def positions(block, lane, hide):
+        away = (block - (me * nb + iota(block.shape, 0))) * BLK + lane % BLK
+        return jnp.where(hide, 1 << 24, away).astype(F32)
+
+    kp_s[0] = positions(block, lane, (block < 0) | late)
+    kp_s[1] = positions(block, lane, block < 0)
+    lane = iota((nb, 2 * picked), 1)
+    late_owner = jnp.where(lane < picked, late_owners[0], late_owners[1])
+    block = jnp.full((nb, 2 * picked), -1, jnp.int32)
+    for e in range(entries):
+        here = (owner[:, e:e + 1] == late_owner) & (rank[:, e:e + 1] == lane // BLK % MOST)
+        block = jnp.where(here, lists[:, e:e + 1], block)
+    late_kp[...] = positions(block, lane, block < 0)
 
     for kind in (2, 3):
         arrive(kind, z, left_col, lambda z, y, hop: z < last)
@@ -385,13 +419,14 @@
         def count(z, y):
             if tile == 1:
                 return (z + (y == N_Y - 1)) + (z + (y >= 1)) + (z + (y >= 2))
+            later = 2 if z >= LATE else 0
+            if tile == 2:
+                return later
             if z == last:
-                return (z + (y == N_Y - 1)) + z + (y >= 1) + (y >= 2)
-            return (z + (y == N_Y - 1)) + (z + (y >= 2))
+                return (z + (y == N_Y - 1)) + z + (y >= 1) + (y >= 2) - later
+            return (z + (y == N_Y - 1)) + (z + (y >= 2)) - later
         return count
 
-    query_row = iota((BLK, keys), 0).astype(F32)
-    ones = jnp.ones((keys, LANES), BF16)
     tile_low = iota((BLK, LANES), 1) < HD
     tile_lane = iota((BLK, LANES), 1)
     core_slope = jnp.where(tp == 0, 1.0, 2.0 ** (-8.0 * heads / n_heads)).astype(F32)
@@ -399,17 +434,29 @@
     def slope_of(head):
         return core_slope * (2.0 ** (-8.0 * (head + 1) / n_heads))
 
-    def attend(r, side):
-        key_pos = kp_s[pl.ds(r, 1), :]
-        allowed = key_pos <= query_row
-        both = jnp.concatenate([kv[side][index_s[side, r, e]] for e in range(entries)], axis=0)
+    def attend(r, side, both, key_pos):
+        count = both.shape[0]
+        allowed = key_pos <= iota((BLK, count), 0).astype(F32)
         scores = dot_nt(q_s[r, side * group * BLK:(side + 1) * group * BLK], both)
         weights = []
         for t in range(group):
             bias = key_pos * (slope_of(side * group + t) * (alibi * LOG2E))
             part = jnp.exp2(scores[t * BLK:(t + 1) * BLK] + bias)
             weights.append(jnp.where(allowed, part, 0.0).astype(BF16))
+        ones = jnp.ones((count, LANES), BF16)
         return dot(jnp.concatenate(weights, axis=0), jnp.concatenate([both, ones], axis=1))
+
+    def attend_chosen(side):
+        for start in range(0, nb, 4):
+            found = []
+            for r in range(start, start + 4):
+                both = jnp.concatenate([kv[side][index_s[side, r, e]] for e in range(entries)], axis=0)
+                found.append(attend(r, side, both, kp_s[side, r:r + 1, :]))
+            for i in range(4):
+                found_s[side, start + i] = found[i]
+
+    def attend_late(r):
+        return attend(r, 0, late_s[...].reshape(2 * picked, LANES), late_kp[r:r + 1, :])
 
     def combine(r, outs):
         sums = jnp.ones((BLK, LANES), F32)
@@ -437,20 +484,20 @@
 
     def one_part(part):
         each = nb // PARTS
-        first = [attend(part * each + i, 0) for i in range(each)]
+        rest = [attend_late(part * each + i) for i in range(each)]
         for i in range(each):
-            combine(part * each + i, (first[i], found_s[part * each + i]))
+            r = part * each + i
+            combine(r, (found_s[0, r] + rest[i], found_s[1, r]))
         at = part_at(part)
         part_send[at] = dot(att_s[at], wo_buf[1]).astype(BF16)
         part_copy(part).start()
 
     index_copy.wait()
+    settle(due(0), end_sem.at[0])
+    attend_chosen(0)
     settle(due(1), end_sem.at[1])
-    for start in range(0, nb, 4):
-        second = [attend(start + i, 1) for i in range(4)]
-        for i in range(4):
-            found_s[start + i] = second[i]
-    settle(due(0), end_sem.at[0])
+    attend_chosen(1)
+    settle(due(2), end_sem.at[2])
     for part in range(PARTS):
         one_part(part)
 
@@ -517,8 +564,10 @@
             vmem((nb, heads * BLK, LANES), BF16),
             vmem((1 + n_kv * nb, BLK, LANES), BF16),
             vmem((1 + n_kv * nb, BLK, LANES), BF16),
-            vmem((nb, entries * BLK), F32),
-            vmem((nb, heads // 2 * BLK, 2 * LANES), F32),
+            vmem((2, MOST, BLK, LANES), BF16),
+            vmem((2, nb, entries * BLK), F32),
+            vmem((nb, 2 * MOST * BLK), F32),
+            vmem((2, nb, heads // 2 * BLK, 2 * LANES), F32),
             vmem((rows, q_cols), BF16),
             vmem((rows, LANES), F32),
             vmem((rows, half), BF16),
@@ -528,7 +577,7 @@
             dma((2, 3)),
             dma((2,)),
             dma((4, n_z)),
-            dma((2,)),
+            dma((3,)),
             dma((2, PARTS)),
         ],
         compiler_params=pltpu.CompilerParams(

time: 32.5 us -> 32.6 us (level)
  no operation moved by 1% of the time
where the time goes in v9:
time: 32.6 us; the launch traced here: 32.1 us
  Pallas kernels  31.4 us (96%)
  between operations  0.64 us (2%)
    pallas_call x1, Pallas kernels, shards(): pl.pallas_call(functools.partial(kernel, n_kv), out_shape=(vmem((rows, ha...  30.7 us
    pallas_call x1, Pallas kernels, shards(): pl.pallas_call(write_out, out_shape=(jax.ShapeDtypeStruct((rows, half), B...  0.72 us

profile of v9, /device:TPU:193, one launch (start us, length us, event | category | flops | bytes accessed | tf_op | source)
XLA Modules:
  0.0 32.1 jit_solution(8678891931045050059)
XLA Ops:
  0.6 30.7 %shard_map.104 = (bf16[256,512]{1,0:T(8,128)(2,1)S(1)}, f32[8,256]{1,0:T(8,128)S(1)}) custom-call(bf16[256,512]{1,0:T(8,128)(2,1)} %bitcast.7, f32[1,1024]{1,0:T(1,128)} %bitcast.8, bf16[1024,512]{1,0:T(8,128)(2,1)} %wq.1, bf16[1024,128]{1,0:T(8,128)(2,1)} %wk.1, bf16[1024,128]{1,0:T(8,128)(2,1)} %wv.1, f32[1,64]{1,0:T(1,128)} %bitcast.10, ...), custom_call_target="tpu_custom_call" | custom-call | tf_op jit(solution)/shard_map/pallas_call | solution.py:543
  31.3 0.7 %shard_map.105 = (bf16[256,512]{1,0:T(8,128)(2,1)}, f32[8,256]{1,0:T(8,128)}) custom-call(bf16[256,512]{1,0:T(8,128)(2,1)S(1)} %get-tuple-element.6.mixed, f32[8,256]{1,0:T(8,128)S(1)} %get-tuple-element.7.log_total), custom_call_target="tpu_custom_call" | custom-call | tf_op jit(solution)/shard_map/pallas_call | solution.py:590

commit v10 on v8

--- a/solution.py
+++ b/solution.py
@@ -435,15 +435,6 @@
             part_send.at[at], part_recv.at[at], part_sem.at[0, part], part_sem.at[1, part],
             device_id={"tp": partner}, device_id_type=MESH)
 
-    def one_part(part):
-        each = nb // PARTS
-        first = [attend(part * each + i, 0) for i in range(each)]
-        for i in range(each):
-            combine(part * each + i, (first[i], found_s[part * each + i]))
-        at = part_at(part)
-        part_send[at] = dot(att_s[at], wo_buf[1]).astype(BF16)
-        part_copy(part).start()
-
     index_copy.wait()
     settle(due(1), end_sem.at[1])
     for start in range(0, nb, 4):
@@ -451,8 +442,13 @@
         for i in range(4):
             found_s[start + i] = second[i]
     settle(due(0), end_sem.at[0])
+    first = [attend(r, 0) for r in range(nb)]
+    for r in range(nb):
+        combine(r, (first[r], found_s[r]))
     for part in range(PARTS):
-        one_part(part)
+        at = part_at(part)
+        part_send[at] = dot(att_s[at], wo_buf[1]).astype(BF16)
+        part_copy(part).start()
 
     own = dot(att_s[...], wo_buf[0])
     row_in = (iota((rows, LANES), 0) % BLK).astype(F32)

time: 32.5 us -> 32.2 us (level)
  no operation moved by 1% of the time
where the time goes in v10:
time: 32.2 us; the launch traced here: 31.9 us
  Pallas kernels  31.3 us (97%)
  between operations  0.64 us (2%)
    pallas_call x1, Pallas kernels, shards(): pl.pallas_call(functools.partial(kernel, n_kv), out_shape=(vmem((rows, ha...  30.6 us
    pallas_call x1, Pallas kernels, shards(): pl.pallas_call(write_out, out_shape=(jax.ShapeDtypeStruct((rows, half), B...  0.72 us

profile of v10, /device:TPU:193, one launch (start us, length us, event | category | flops | bytes accessed | tf_op | source)
XLA Modules:
  0.0 31.9 jit_solution(16462593608339990947)
XLA Ops:
  0.6 30.6 %shard_map.104 = (bf16[256,512]{1,0:T(8,128)(2,1)S(1)}, f32[8,256]{1,0:T(8,128)S(1)}) custom-call(bf16[256,512]{1,0:T(8,128)(2,1)} %bitcast.7, f32[1,1024]{1,0:T(1,128)} %bitcast.8, bf16[1024,512]{1,0:T(8,128)(2,1)} %wq.1, bf16[1024,128]{1,0:T(8,128)(2,1)} %wk.1, bf16[1024,128]{1,0:T(8,128)(2,1)} %wv.1, f32[1,64]{1,0:T(1,128)} %bitcast.10, ...), custom_call_target="tpu_custom_call" | custom-call | tf_op jit(solution)/shard_map/pallas_call | solution.py:492
  31.2 0.7 %shard_map.105 = (bf16[256,512]{1,0:T(8,128)(2,1)}, f32[8,256]{1,0:T(8,128)}) custom-call(bf16[256,512]{1,0:T(8,128)(2,1)S(1)} %get-tuple-element.6.mixed, f32[8,256]{1,0:T(8,128)S(1)} %get-tuple-element.7.log_total), custom_call_target="tpu_custom_call" | custom-call | tf_op jit(solution)/shard_map/pallas_call | solution.py:537

commit v11 on v10

--- a/solution.py
+++ b/solution.py
@@ -131,17 +131,13 @@
 
     def place_copy(direction, slot):
         return pltpu.make_async_remote_copy(
-            place_send, place_recv.at[slot], place_sem.at[0, slot], place_sem.at[1, slot],
+            place_send, place_recv.at[slot], place_sem.at[0], place_sem.at[1],
             device_id={"kv": neighbour[direction]}, device_id_type=MESH)
 
     place_copies = [place_copy(RIGHT, 0), place_copy(LEFT, 1), place_copy(FAR, 2)]
     for copy in place_copies:
         copy.start()
 
-    for side, which in ((0, tp), (1, partner)):
-        for head in range(heads):
-            to = head % group * LANES + head // group * HD
-            load(OUT, (wo.at[head * HD:(head + 1) * HD, span(which)], wo_buf.at[side, to:to + HD]))
 
     loaded(GAIN, g_buf)
     loaded(W0, w_buf.at[0])
@@ -237,9 +233,9 @@
             left_s[row, 1] = found[MOST:2 * MOST]
             right_s[row, 1] = found[2 * MOST:]
 
-        send_chosen(FAR, far_s.at[row, 1], 1, row, y, to_far, hop)
         send_chosen(LEFT, left_s.at[row, 1], 1, row, y, to_left, hop)
         send_chosen(RIGHT, right_s.at[row, 1], 1, row, y, to_right, hop)
+        send_chosen(FAR, far_s.at[row, 1], 1, row, y, to_far, hop)
 
     def choose_0(row, to_left, hop=None):
         @pl.when(to_left(z, y, hop))
@@ -273,8 +269,13 @@
         send_whole(UP, kind, z, y, lambda z, y, hop: z < last)
         send_whole(DOWN, kind, z, y, lambda z, y, hop: z < back_a)
 
-    for copy in place_copies:
-        copy.wait()
+    for side, which in ((0, tp), (1, partner)):
+        for head in range(heads):
+            to = head % group * LANES + head // group * HD
+            load(OUT, (wo.at[head * HD:(head + 1) * HD, span(which)], wo_buf.at[side, to:to + HD]))
+
+    for sem in range(2):
+        pltpu.make_async_copy(place_recv, place_recv, place_sem.at[sem]).wait()
     spread = jnp.where(
         iota((n_blocks, rows), 0) % nb == iota((n_blocks, rows), 1) // BLK, 1.0, 0.0).astype(BF16)
     row_owner = iota((n_z, n_blocks), 0) * N_Y
@@ -521,7 +522,7 @@
             vmem((rows, half), BF16),
             dma((8,)),
             dma((2,)),
-            dma((2, 3)),
+            dma((2,)),
             dma((2,)),
             dma((4, n_z)),
             dma((2,)),

time: 32.2 us -> 32.2 us (level)
  no operation moved by 1% of the time
where the time goes in v11:
time: 32.2 us; the launch traced here: 31.9 us
  Pallas kernels  31.3 us (97%)
  between operations  0.64 us (2%)
    pallas_call x1, Pallas kernels, shards(): pl.pallas_call(functools.partial(kernel, n_kv), out_shape=(vmem((rows, ha...  30.5 us
    pallas_call x1, Pallas kernels, shards(): pl.pallas_call(write_out, out_shape=(jax.ShapeDtypeStruct((rows, half), B...  0.72 us

profile of v11, /device:TPU:193, one launch (start us, length us, event | category | flops | bytes accessed | tf_op | source)
XLA Modules:
  0.0 31.9 jit_solution(587406315290501209)
XLA Ops:
  0.6 30.5 %shard_map.104 = (bf16[256,512]{1,0:T(8,128)(2,1)S(1)}, f32[8,256]{1,0:T(8,128)S(1)}) custom-call(bf16[256,512]{1,0:T(8,128)(2,1)} %bitcast.7, f32[1,1024]{1,0:T(1,128)} %bitcast.8, bf16[1024,512]{1,0:T(8,128)(2,1)} %wq.1, bf16[1024,128]{1,0:T(8,128)(2,1)} %wk.1, bf16[1024,128]{1,0:T(8,128)(2,1)} %wv.1, f32[1,64]{1,0:T(1,128)} %bitcast.10, ...), custom_call_target="tpu_custom_call" | custom-call | tf_op jit(solution)/shard_map/pallas_call | solution.py:493
  31.2 0.7 %shard_map.105 = (bf16[256,512]{1,0:T(8,128)(2,1)}, f32[8,256]{1,0:T(8,128)}) custom-call(bf16[256,512]{1,0:T(8,128)(2,1)S(1)} %get-tuple-element.6.mixed, f32[8,256]{1,0:T(8,128)S(1)} %get-tuple-element.7.log_total), custom_call_target="tpu_custom_call" | custom-call | tf_op jit(solution)/shard_map/pallas_call | solution.py:538
